TPU v7x, 128 devices: a whole 4x4x4 slice. The times are simulated.
128 devices in a mesh: ep: 32 (over z, y, core), tp: 4 (over x).
Axes of the slice: x: 4, y: 4, z: 4, core: 2. Of those that a mesh axis runs over, the one named last changes fastest.
Arguments:
- mixer_microbatch: bfloat16 [32768, 2048], P(('ep', 'tp')), may hold values from -6 to 6
- mixer_gain_vector: float32 [2048], replicated, may hold values from 0.1 to 1.9
- asker_matrix: bfloat16 [2048, 1024], P(None, 'tp'), may hold values from -0.125 to 0.125
- matcher_matrix: bfloat16 [2048, 1024], P(None, 'tp'), may hold values from -0.125 to 0.125
- fading_matrix: bfloat16 [2048, 1024], P(None, 'tp'), may hold values from -0.125 to 0.125
- content_matrix: bfloat16 [2048, 2048], P(None, 'tp'), may hold values from -0.125 to 0.125
- result_valve_matrix: bfloat16 [2048, 2048], P(None, 'tp'), may hold values from -0.125 to 0.125
- fading_shift_vector: float32 [1024], P('tp'), may hold values from -1.5 to 20
- extra_fade_amount: float32 [32768, 16], P('ep', 'tp'), may hold values from -0.7 to 0
- starting_memory: float32 [1024, 128], P('tp'), may hold values from -24 to 24
- subspace_gain_vector: float32 [2048], P('tp'), may hold values from 0.1 to 1.9
- result_matrix: bfloat16 [2048, 2048], replicated, may hold values from -0.125 to 0.125
- specialist_microbatch: bfloat16 [16384, 2048], P(('ep', 'tp')), may hold values from -6 to 6
- specialist_gain_vector: float32 [2048], replicated, may hold values from 0.1 to 1.9
- picked_specialists: int32 [16384, 2], P(('ep', 'tp')), may hold values from 0 to 63, all different within a row; in each aligned block of 128 rows (0 to 127, 128 to 255, ...) at most 6 rows name the same one
- specialist_mixing_factor: float32 [16384, 2], P(('ep', 'tp')), may hold values from 0.3 to 1.5
- specialist_valve_matrix: bfloat16 [64, 2048, 1024], P('ep', None, 'tp'), may hold values from -0.125 to 0.125
- specialist_widen_matrix: bfloat16 [64, 2048, 1024], P('ep', None, 'tp'), may hold values from -0.125 to 0.125
- specialist_shrink_matrix: bfloat16 [64, 1024, 2048], P('ep', 'tp'), may hold values from -0.1875 to 0.1875
- joint_valve_matrix: bfloat16 [2048, 512], P(None, 'tp'), may hold values from -0.125 to 0.125
- joint_widen_matrix: bfloat16 [2048, 512], P(None, 'tp'), may hold values from -0.125 to 0.125
- joint_shrink_matrix: bfloat16 [512, 2048], P('tp'), may hold values from -0.25 to 0.25
Outputs:
- mixer_sublayer_result: bfloat16 [32768, 2048], P(('ep', 'tp'))
- moe_out: bfloat16 [16384, 2048], P(('ep', 'tp'))
Inputs may be any that keep to these rules, and one draw needn't show every extreme that they name: `picked_specialists`: each row names 2 different experts; among the rows of one device no expert is named more than 6 times.
All inputs are finite; a program needn't handle non-finite values.
Results may differ from a plain program's by a relative error of at most 0.025.
Values may be sent and summed in bfloat16 or wider, within the bound.
A program may use at most 192 MiB of HBM per device.

v0:
```python
import functools
import jax
import jax.numpy as jnp
from jax import lax
from jax.experimental import pallas as pl
from jax.experimental.pallas import tpu as pltpu
from jax.sharding import PartitionSpec as P

NORM_EPS = 1e-06
F32 = jnp.float32
BF16 = jnp.bfloat16
MESH = pl.DeviceIdType.MESH
EXACT = lax.Precision.HIGHEST
CHUNKS = 4
SPAN = 64


def rms(values, gain):
    wide = values.astype(F32)
    scale = lax.rsqrt(jnp.mean(wide * wide, axis=-1, keepdims=True) + NORM_EPS)
    return (wide * scale * gain).astype(BF16)


def at(start, size, unit=None):
    return pl.ds(pl.multiple_of(start, unit or size), size)


def layer_kernel(
    shape,
    xa_hbm, ga_ref, wq_hbm, wk_hbm, wf_hbm, wc_hbm, wg_hbm, shift_ref, fade_ref, first_ref,
    hgain_ref, wr_hbm,
    x_hbm, gain_ref, meta_ref, wv_hbm, wu_hbm, wd_hbm, jv_hbm, ju_hbm, jd_hbm,
    mix_out, moe_out,
    xa, na, wa, pj, att, qg, state, sent, heard, pt,
    x_ref, wv, wu, wd, jv, ju, jd,
    gm, metas, onehot, weigh, tx, rx, hid, ry, shid, fx,
    wsem, ags, agr, ms, mr, dts, drs, dls, rts, rrs, rls, fs, fr,
    aas, aar, ss, sr, hs, hr,
):
    n_ep, n_tp, tok, width, slots, ffe, seg, kw, vw = shape
    per = n_tp * 2 * slots
    rows = n_ep * per
    wc = width // CHUNKS
    part_rows = 512
    heads = vw // 128
    segrows = seg * n_tp
    quarter = seg // 4
    ep = lax.axis_index("ep")
    tp = lax.axis_index("tp")
    core, yy, zz = lax.rem(ep, 2), lax.rem(ep // 2, 4), ep // 8
    right = lax.rem(tp + 1, n_tp)
    left = lax.rem(tp + n_tp - 1, n_tp)
    across = lax.rem(tp + 2, n_tp)

    def peer(i):
        return (
            lax.rem(zz + i // 8, 4) * 8
            + lax.rem(yy + lax.rem(i // 2, 4), 4) * 2
            + lax.rem(core + lax.rem(i, 2), 2)
        )

    pairs = [
        (x_hbm, x_ref), (xa_hbm, xa),
        (wq_hbm, wa.at[:, 0:kw]), (wk_hbm, wa.at[:, kw : 2 * kw]), (wf_hbm, wa.at[:, 2 * kw : 3 * kw]),
        (wc_hbm, wa.at[:, 3 * kw : 3 * kw + vw]), (wg_hbm, wa.at[:, 3 * kw + vw : 3 * kw + 2 * vw]),
        (jv_hbm, jv), (ju_hbm, ju), (wv_hbm, wv), (wu_hbm, wu), (wd_hbm, wd), (jd_hbm, jd),
    ]
    loads = [pltpu.make_async_copy(s, d, wsem.at[i]) for i, (s, d) in enumerate(pairs)]
    for copy in loads:
        copy.start()

    barrier = pltpu.get_barrier_semaphore()

    def greet(i, carry):
        pl.semaphore_signal(barrier, inc=1, device_id={"ep": peer(i)}, device_id_type=MESH)
        return carry

    lax.fori_loop(1, n_ep, greet, 0)
    for step in range(1, n_tp):
        pl.semaphore_signal(
            barrier, inc=1, device_id={"tp": lax.rem(tp + step, n_tp)}, device_id_type=MESH
        )

    loads[0].wait()
    normed = rms(x_ref[...], gain_ref[...])
    mine = at(tp * tok, tok)
    for c in range(CHUNKS):
        gm[c, mine, :] = normed[:, c * wc : (c + 1) * wc]

    meta = meta_ref[...]
    tall = jnp.concatenate([meta, jnp.zeros((tok - 8, tok), F32)], axis=0).T
    before = lax.broadcasted_iota(jnp.int32, (tok, tok), 0) < lax.broadcasted_iota(
        jnp.int32, (tok, tok), 1
    )
    names = meta[0:2].astype(jnp.int32)
    tall_names = tall[:, 0:2].astype(jnp.int32)
    spots = []
    for k in range(2):
        row = names[k : k + 1]
        hits = jnp.zeros((tok, tok), F32)
        for j in range(2):
            hits = hits + jnp.where((tall_names[:, j : j + 1] == row) & before, 1.0, 0.0)
        rank = jnp.sum(hits, axis=0, keepdims=True)
        local = row // 2
        base = (local * per + tp * 2 * slots + (row - 2 * local) * slots).astype(F32)
        spots.append(base + rank)
    metas[at(tp * 8, 8), :] = jnp.concatenate(
        [spots[0], spots[1], meta[2:4], jnp.zeros((4, tok), F32)], axis=0
    )

    pl.semaphore_wait(barrier, n_ep - 1 + n_tp - 1)

    my_meta = metas.at[at(tp * 8, 8)]
    sends = []

    def send_tp(src, dst, ssem, rsem, to):
        copy = pltpu.make_async_remote_copy(
            src_ref=src, dst_ref=dst, send_sem=ssem, recv_sem=rsem,
            device_id={"tp": to}, device_id_type=MESH,
        )
        copy.start()
        sends.append(copy)

    def arrived(ref, sem):
        pltpu.make_async_copy(ref, ref, sem).wait()

    for step in range(1, n_tp):
        send_tp(my_meta, my_meta, ms.at[step], mr.at[step], lax.rem(tp + step, n_tp))

    def block(c, who, half=None):
        if half is None:
            return gm.at[c, at(who * tok, tok)]
        return gm.at[c, at(who * tok + half * (tok // 2), tok // 2)]

    for c in range(CHUNKS):
        own = block(c, tp)
        send_tp(own, own, ags.at[c, 0], agr.at[c, 0], right)
        send_tp(own, own, ags.at[c, 1], agr.at[c, 1], left)

    loads[1].wait()
    for i in range(4):
        r = slice(i * quarter, (i + 1) * quarter)
        na[at(tp * seg + i * quarter, quarter), :] = rms(xa[r, :], ga_ref[...])

    def ablock(who, i):
        return na.at[at(who * seg + i * quarter, quarter)]

    def attention_send(i):
        own = ablock(tp, i)
        send_tp(own, own, aas.at[0, i], aar.at[0, i], right)
        send_tp(own, own, aas.at[1, i], aar.at[1, i], left)

    for step in range(1, n_tp):
        arrived(metas.at[at(lax.rem(tp + n_tp - step, n_tp) * 8, 8)], mr.at[step])

    def table(t, carry):
        r0 = pl.multiple_of(t * 256, 256)
        ids = lax.broadcasted_iota(jnp.int32, (256, tok), 0) + r0
        for m in range(n_tp):
            spot = metas[8 * m : 8 * m + 2, :].astype(jnp.int32)
            hit = (ids == spot[0:1]) | (ids == spot[1:2])
            onehot[pl.ds(r0, 256), m * tok : (m + 1) * tok] = jnp.where(hit, 1.0, 0.0).astype(BF16)
        return carry

    lax.fori_loop(0, rows // 256, table, 0)

    def local_rows(c, src, dst, sem):
        own = at(ep * per, per)
        return pltpu.make_async_copy(src.at[c, own], dst.at[c, own], sem.at[c])

    def spread(c, src, dst, ssem, rsem):
        def one(i, carry):
            to = peer(i)
            pltpu.make_async_remote_copy(
                src_ref=src.at[c, at(to * per, per)],
                dst_ref=dst.at[c, at(ep * per, per)],
                send_sem=ssem.at[c], recv_sem=rsem.at[c],
                device_id={"ep": to}, device_id_type=MESH,
            ).start()
            return carry

        lax.fori_loop(1, n_ep, one, 0)
        local_rows(c, src, dst, dls if src is tx and dst is rx else rls).start()

    def all_but_one(ref, c, sem):
        some = ref.at[c, pl.ds(0, rows - per)]
        pltpu.make_async_copy(some, some, sem.at[c]).wait()

    def project(who):
        r = at(who * seg, seg)

        def one(n, carry):
            cols = at(n * 256, 256)
            pj[r, cols] = jnp.dot(na[r, :], wa[:, cols], preferred_element_type=F32).astype(BF16)
            return carry

        lax.fori_loop(0, (3 * kw + 2 * vw) // 256, one, 0)

    for c in range(CHUNKS):
        arrived(block(c, left), agr.at[c, 0])
        fwd = block(c, left, 0)
        send_tp(fwd, fwd, ags.at[c, 2], agr.at[c, 2], right)
        arrived(block(c, right), agr.at[c, 1])
        fwd = block(c, right, 1)
        send_tp(fwd, fwd, ags.at[c, 3], agr.at[c, 3], left)
        attention_send(c)
        arrived(block(c, across, 0), agr.at[c, 2])
        arrived(block(c, across, 1), agr.at[c, 3])

        def build(t, carry, c=c):
            r = at(t * part_rows, part_rows)
            tx[c, r, :] = jnp.dot(onehot[r, :], gm[c], preferred_element_type=F32).astype(BF16)
            return carry

        lax.fori_loop(0, rows // part_rows, build, 0)
        spread(c, tx, rx, dts, drs)
        if c == 0:
            for copy in loads[2:7]:
                copy.wait()
            project(tp)

    for i in range(4):
        arrived(ablock(left, i), aar.at[0, i])
        if i < 2:
            fwd = ablock(left, i)
            send_tp(fwd, fwd, aas.at[2, i], aar.at[2, i], right)
        arrived(ablock(right, i), aar.at[1, i])
        if i >= 2:
            fwd = ablock(right, i)
            send_tp(fwd, fwd, aas.at[2, i], aar.at[2, i], left)
    project(left)
    project(right)

    loads[7].wait()
    loads[8].wait()

    def shared(t, carry):
        r = at(t * tok, tok)
        g = jnp.zeros((tok, jv.shape[1]), F32)
        u = jnp.zeros((tok, jv.shape[1]), F32)
        for c in range(CHUNKS):
            xs = gm[c, r, :]
            g = g + jnp.dot(xs, jv[c * wc : (c + 1) * wc, :], preferred_element_type=F32)
            u = u + jnp.dot(xs, ju[c * wc : (c + 1) * wc, :], preferred_element_type=F32)
        shid[r, :] = (jax.nn.silu(g) * u).astype(BF16)
        return carry

    lax.fori_loop(0, n_tp, shared, 0)

    def weights(m, carry):
        both = jnp.concatenate([metas[at(8 * m, 8), :], jnp.zeros((tok - 8, tok), F32)], axis=0).T
        spot = both[:, 0:2].astype(jnp.int32)
        for c in range(rows // 256):
            ids = lax.broadcasted_iota(jnp.int32, (tok, 256), 1) + c * 256
            w = jnp.where(ids == spot[:, 0:1], both[:, 2:3], 0.0) + jnp.where(
                ids == spot[:, 1:2], both[:, 3:4], 0.0
            )
            weigh[at(m * tok, tok), c * 256 : (c + 1) * 256] = w.astype(BF16)
        return carry

    lax.fori_loop(0, n_tp, weights, 0)

    for i in range(4):
        arrived(ablock(across, i), aar.at[2, i])
    project(across)
    late_load = pltpu.make_async_copy(wr_hbm, wa, wsem.at[13])
    late_load.start()

    state[...] = jnp.zeros_like(state)

    def iota(dims, axis):
        return lax.broadcasted_iota(jnp.int32, dims, axis)

    lower = jnp.where(iota((SPAN, SPAN), 0) >= iota((SPAN, SPAN), 1), 1.0, 0.0)
    causal = iota((SPAN, kw), 0) >= lax.rem(iota((SPAN, kw), 1), SPAN)
    head_of = iota((SPAN, kw), 1) // 64
    kmask = jnp.where(iota((kw, kw), 0) // 64 == iota((kw, kw), 1) // 64, 1.0, 0.0).astype(BF16)
    vmask = jnp.where(iota((kw, vw), 0) // 64 == iota((kw, vw), 1) // 128, 1.0, 0.0)
    vmask16 = vmask.astype(BF16)

    def span(n, carry):
        past, past_tall = carry
        r = at(n * SPAN, SPAN)
        q = pj[r, 0:kw].astype(F32) * 0.125
        k = pj[r, kw : 2 * kw].astype(F32)
        z = pj[r, 2 * kw : 3 * kw].astype(F32) + shift_ref[...]
        v = pj[r, 3 * kw : 3 * kw + vw]
        extra = fade_ref[r, :]
        add = extra[:, 0:1]
        for h in range(1, heads):
            add = jnp.where(head_of == h, extra[:, h : h + 1], add)
        rate = (jnp.minimum(z, 0.0) - jnp.log1p(jnp.exp(-jnp.abs(z)))) * 0.0625 + add
        running = jnp.dot(lower, rate, precision=EXACT, preferred_element_type=F32)
        total = running[SPAN - 1 : SPAN]
        qf = q * jnp.exp(running)
        kd = (k * jnp.exp(-running)).astype(BF16)
        ku = (k * jnp.exp(total - running)).astype(BF16)
        qg[r, :] = (qf * jnp.exp(past)).astype(BF16)
        qf = qf.astype(BF16)
        wide_k = jnp.concatenate([kd] * heads, axis=0) * kmask
        scores = lax.dot_general(qf, wide_k, (((1,), (1,)), ((), ())), preferred_element_type=F32)
        scores = jnp.where(causal, scores, 0.0).astype(BF16)
        wide_v = jnp.concatenate([v] * heads, axis=0) * vmask16
        held = state[...]
        att[r, :] = jnp.dot(scores, wide_v, preferred_element_type=F32) + jnp.dot(
            qf, held.astype(BF16), preferred_element_type=F32
        )
        grown = lax.dot_general(ku, v, (((0,), (0,)), ((), ())), preferred_element_type=F32)
        tall_total = lax.dot_general(
            rate, jnp.ones((SPAN, 128), F32), (((0,), (0,)), ((), ())),
            precision=EXACT, preferred_element_type=F32,
        )
        fade = jnp.exp(tall_total)
        state[...] = jnp.concatenate([fade] * heads, axis=1) * held + grown * vmask
        return past + total, past_tall + tall_total

    _, whole = lax.fori_loop(
        0, segrows // SPAN, span, (jnp.zeros((1, kw), F32), jnp.zeros((kw, 128), F32))
    )
    own_fade = jnp.exp(whole)
    own_state = jnp.concatenate(
        [state[64 * h : 64 * h + 64, 128 * h : 128 * h + 128] for h in range(heads)], axis=0
    )

    def put(level, fade, held):
        sent[level, 0] = fade.astype(BF16)
        sent[level, 1] = held.astype(BF16)

    def share(level, slot, to):
        pltpu.make_async_remote_copy(
            src_ref=sent.at[level], dst_ref=heard.at[slot], send_sem=ss.at[slot], recv_sem=sr.at[slot],
            device_id={"ep": to}, device_id_type=MESH,
        ).start()

    def hear(level, slot):
        arrived(heard.at[slot], sr.at[slot])
        pltpu.make_async_copy(sent.at[level], sent.at[level], ss.at[slot]).wait()

    def after(first, second):
        return first[0] * second[0], second[0] * first[1] + second[1]

    def pick(flag, pair, other):
        return tuple(jnp.where(flag, a, b) for a, b in zip(pair, other))

    neutral = (jnp.ones((kw, 128), F32), jnp.zeros((kw, 128), F32))

    def load_pair(slot):
        return heard[slot, 0].astype(F32), heard[slot, 1].astype(F32)

    def ring_fold(base, place, me):
        prefix, everything = neutral, neutral
        rounded = tuple(a.astype(BF16).astype(F32) for a in me)
        for j in range(4):
            there = rounded
            for d in range(1, 4):
                there = pick(lax.rem(place + 4 - d, 4) == j, load_pair(base + d - 1), there)
            everything = after(everything, there)
            prefix = pick(place > j, after(prefix, there), prefix)
        return prefix, everything

    put(0, own_fade, own_state)
    share(0, 0, zz * 8 + yy * 2 + (1 - core))

    def level_one():
        hear(0, 0)
        mate = load_pair(0)
        me = (sent[0, 0].astype(F32), sent[0, 1].astype(F32))
        low, high = pick(core == 0, me, mate), pick(core == 0, mate, me)
        chip = after(low, high)
        put(1, *chip)
        for d in range(1, 4):
            share(1, d, zz * 8 + lax.rem(yy + d, 4) * 2 + core)
        return pick(core == 0, neutral, mate), chip

    def level_two(chip):
        for d in range(1, 4):
            hear(1, d)
        prefix, column = ring_fold(1, yy, chip)
        put(2, *column)
        for d in range(1, 4):
            share(2, 3 + d, lax.rem(zz + d, 4) * 8 + yy * 2 + core)
        return prefix, column

    def level_three(column):
        for d in range(1, 4):
            hear(2, 3 + d)
        return ring_fold(4, zz, column)[0]

    in_chip, chip = level_one()

    for copy in loads[9:11]:
        copy.wait()
    for c in range(CHUNKS):
        local_rows(c, tx, rx, dls).wait()
        all_but_one(rx, c, drs)

    in_column, column = level_two(chip)

    def expert(t, carry):
        r = at(t * part_rows, part_rows)
        late = lax.rem(lax.broadcasted_iota(jnp.int32, (part_rows, ffe), 0) + t * part_rows, 2 * slots) >= slots
        for l in range(2):
            g = jnp.zeros((part_rows, ffe), F32)
            u = jnp.zeros((part_rows, ffe), F32)
            for c in range(CHUNKS):
                xs = rx[c, r, :]
                g = g + jnp.dot(xs, wv[l, c * wc : (c + 1) * wc, :], preferred_element_type=F32)
                u = u + jnp.dot(xs, wu[l, c * wc : (c + 1) * wc, :], preferred_element_type=F32)
            h = jax.nn.silu(g) * u
            h = jnp.where(late, h, 0.0) if l else jnp.where(late, 0.0, h)
            hid[r, l * ffe : (l + 1) * ffe] = h.astype(BF16)
        return carry

    lax.fori_loop(0, rows // part_rows, expert, 0)
    in_slice = level_three(column)
    earlier = after(after(in_slice, in_column), in_chip)

    loads[11].wait()
    for c in range(CHUNKS):
        all_but_one(tx, c, dts)

        def down(t, carry, c=c):
            r = at(t * part_rows, part_rows)
            tx[c, r, :] = jnp.dot(
                hid[r, :], wd[:, c * wc : (c + 1) * wc], preferred_element_type=F32
            ).astype(BF16)
            return carry

        lax.fori_loop(0, rows // part_rows, down, 0)
        spread(c, tx, ry, rts, rrs)

    entering = earlier[1] + earlier[0] * first_ref[...]
    wide_entry = jnp.concatenate([entering.astype(BF16)] * heads, axis=1) * vmask16
    for step in range(n_tp):
        who = lax.rem(tp + step + 1, n_tp)

        def finish(i, carry, who=who):
            r = at(who * seg + i * 128, 128)
            full = att[r, :] + jnp.dot(qg[r, :], wide_entry, preferred_element_type=F32)
            for h in range(heads):
                a = full[:, 128 * h : 128 * h + 128]
                scale = lax.rsqrt(jnp.mean(a * a, axis=-1, keepdims=True) + NORM_EPS)
                g = pj[r, 3 * kw + vw + 128 * h : 3 * kw + vw + 128 * h + 128].astype(F32)
                gain = hgain_ref[:, 128 * h : 128 * h + 128]
                pj[r, 128 * h : 128 * h + 128] = (a * scale * gain * jax.nn.silu(g)).astype(BF16)
            return carry

        lax.fori_loop(0, seg // 128, finish, 0)
        if step < n_tp - 1:
            send_tp(pj.at[at(who * seg, seg), 0:vw], pt.at[step], hs.at[step], hr.at[step], who)

    late_load.wait()
    from_self = pj[at(tp * seg, seg), 0:vw]
    for step in range(n_tp - 1):
        arrived(pt.at[step], hr.at[step])

    def result(n, carry):
        cols = at(n * 512, 512)
        got = jnp.dot(from_self, wa[at(tp * vw, vw), cols], preferred_element_type=F32)
        for step in range(n_tp - 1):
            source = lax.rem(tp + n_tp - step - 1, n_tp)
            got = got + jnp.dot(pt[step], wa[at(source * vw, vw), cols], preferred_element_type=F32)
        mix_out[:, cols] = got.astype(BF16)
        return carry

    lax.fori_loop(0, width // 512, result, 0)

    for copy in sends:
        copy.wait_send()

    loads[12].wait()
    last = []
    for c in range(CHUNKS):
        local_rows(c, tx, ry, rls).wait()
        all_but_one(ry, c, rrs)

        def combine(m, carry, c=c):
            r = at(m * 256, 256)
            got = jnp.dot(weigh[r, :], ry[c], preferred_element_type=F32)
            got = got + jnp.dot(shid[r, :], jd[:, c * wc : (c + 1) * wc], preferred_element_type=F32)
            gm[c, r, :] = got.astype(BF16)
            return carry

        lax.fori_loop(0, n_tp * tok // 256, combine, 0)
        for step in range(1, n_tp):
            to = lax.rem(tp + step, n_tp)
            copy = pltpu.make_async_remote_copy(
                src_ref=gm.at[c, at(to * tok, tok)],
                dst_ref=fx.at[c, step - 1],
                send_sem=fs.at[c, step], recv_sem=fr.at[c, step],
                device_id={"tp": to}, device_id_type=MESH,
            )
            copy.start()
            last.append(copy)

    for c in range(CHUNKS):
        total = gm[c, mine, :].astype(F32)
        for step in range(1, n_tp):
            last[c * (n_tp - 1) + step - 1].wait()
            total = total + fx[c, step - 1].astype(F32)
        moe_out[:, c * wc : (c + 1) * wc] = total.astype(BF16)
        all_but_one(tx, c, rts)


def body(
    xa, ga, wq, wk, wf, wc_, wg, shift, fade, first, hgain, wr,
    x, gain, picked, mixing, wv, wu, wd, jv, ju, jd,
):
    n_ep, n_tp = lax.axis_size("ep"), lax.axis_size("tp")
    tok, width = x.shape
    seg = xa.shape[0]
    kw, vw = wq.shape[1], wc_.shape[1]
    local, _, ffe = wv.shape
    slots = 3 * tok * 2 // (2 * n_ep * local)
    rows = n_ep * n_tp * 2 * slots
    wc = width // CHUNKS
    meta = jnp.concatenate([picked.T.astype(F32), mixing.T, jnp.zeros((4, tok), F32)], axis=0)
    hbm = pl.BlockSpec(memory_space=pl.ANY)
    vmem = pl.BlockSpec(memory_space=pltpu.VMEM)
    dma = pltpu.SemaphoreType.DMA
    V = pltpu.VMEM
    return pl.pallas_call(
        functools.partial(layer_kernel, (n_ep, n_tp, tok, width, slots, ffe, seg, kw, vw)),
        out_shape=(
            jax.ShapeDtypeStruct((seg, width), BF16),
            jax.ShapeDtypeStruct((tok, width), BF16),
        ),
        in_specs=[hbm, vmem] + [hbm] * 5 + [vmem] * 4 + [hbm] + [hbm, vmem, vmem] + [hbm] * 6,
        out_specs=(vmem, vmem),
        scratch_shapes=[
            V((seg, width), BF16),
            V((seg * n_tp, width), BF16),
            V((width, width), BF16),
            V((seg * n_tp, 3 * kw + 2 * vw), BF16),
            V((seg * n_tp, vw), F32),
            V((seg * n_tp, kw), BF16),
            V((kw, vw), F32),
            V((3, 2, kw, 128), BF16),
            V((7, 2, kw, 128), BF16),
            V((n_tp - 1, seg, vw), BF16),
            V((tok, width), BF16), V(wv.shape, BF16), V(wu.shape, BF16), V((2 * ffe, width), BF16),
            V(jv.shape, BF16), V(ju.shape, BF16), V(jd.shape, BF16),
            V((CHUNKS, n_tp * tok, wc), BF16),
            V((8 * n_tp, tok), F32),
            V((rows, n_tp * tok), BF16),
            V((n_tp * tok, rows), BF16),
            V((CHUNKS, rows, wc), BF16),
            V((CHUNKS, rows, wc), BF16),
            V((rows, 2 * ffe), BF16),
            V((CHUNKS, rows, wc), BF16),
            V((n_tp * tok, jv.shape[1]), BF16),
            V((CHUNKS, n_tp - 1, tok, wc), BF16),
            dma((14,)), dma((CHUNKS, 4)), dma((CHUNKS, 4)), dma((n_tp,)), dma((n_tp,)),
            dma((CHUNKS,)), dma((CHUNKS,)), dma((CHUNKS,)),
            dma((CHUNKS,)), dma((CHUNKS,)), dma((CHUNKS,)),
            dma((CHUNKS, n_tp)), dma((CHUNKS, n_tp)),
            dma((3, 4)), dma((3, 4)), dma((7,)), dma((7,)), dma((n_tp,)), dma((n_tp,)),
        ],
        compiler_params=pltpu.CompilerParams(
            collective_id=0, has_side_effects=True, vmem_limit_bytes=67043328
        ),
        name="layer",
    )(
        xa, ga.reshape(1, -1), wq, wk, wf, wc_, wg, shift.reshape(1, -1), fade, first,
        hgain.reshape(1, -1), wr,
        x, gain.reshape(1, -1), meta, wv, wu, wd.reshape(2 * ffe, width), jv, ju, jd,
    )


def solution(mesh):
    return jax.shard_map(
        body,
        mesh=mesh,
        in_specs=(
            P(("ep", "tp"), None),
            P(),
            P(None, "tp"),
            P(None, "tp"),
            P(None, "tp"),
            P(None, "tp"),
            P(None, "tp"),
            P("tp"),
            P("ep", "tp"),
            P("tp", None),
            P("tp"),
            P(),
            P(("ep", "tp"), None),
            P(),
            P(("ep", "tp"), None),
            P(("ep", "tp"), None),
            P("ep", None, "tp"),
            P("ep", None, "tp"),
            P("ep", "tp", None),
            P(None, "tp"),
            P(None, "tp"),
            P("tp", None),
        ),
        out_specs=(P(("ep", "tp"), None), P(("ep", "tp"), None)),
        check_vma=False,
    )
```

profile of v0, /device:TPU:0, one launch (start us, length us, event | category | flops | bytes accessed | tf_op | source)
XLA Modules:
  0.0 208.5 jit_solution(11516764409919543245)
XLA Ops:
  0.6 0.1 pad.2.clone
  0.7 0.7 convert_bitcast_fusion
  1.4 1.3 maximum_maximum_fusion.meta_ref
  2.7 1.7 copy.24.fade_ref
  4.5 200.8 %layer.1 = (bf16[256,2048]{1,0:T(8,128)(2,1)}, bf16[128,2048]{1,0:T(8,128)(2,1)}) custom-call(bf16[256,2048]{1,0:T(8,128)(2,1)} %xa_hbm.1, f32[1,2048]{1,0:T(1,128)} %bitcast.9, bf16[2048,256]{1,0:T(8,128)(2,1)} %wq_hbm.1, bf16[2048,256]{1,0:T(8,128)(2,1)} %wk_hbm.1, bf16[2048,256]{1,0:T(8,128)(2,1)} %wf_hbm.1, bf16[2048,512]{1,0:T(8,128)(2,1)} %wc_hbm.1, ...), custom_call_target="tpu_custom_call" | custom-call | tf_op jit(solution)/shard_map/layer/pallas_call | solution.py:522
  205.3 0.0 copy-start
  205.3 2.4 %copy.27 = bf16[256,2048]{1,0:T(8,128)(2,1)} copy(bf16[256,2048]{1,0:T(8,128)(2,1)} %get-tuple-element.4) | data formatting | bytes 2097152
  207.7 0.0 copy-done
  207.7 0.8 copy.28
  (1 shorter events, 0.0 us)
Async XLA Ops:
  205.3 2.4 %copy-start = (bf16[128,2048]{1,0:T(8,128)(2,1)S(1)}, bf16[128,2048]{1,0:T(8,128)(2,1)}, u32[]{:S(2)}) copy-start(bf16[128,2048]{1,0:T(8,128)(2,1)} %get-tuple-element.5) | copy-start | bytes 1572868
where the time goes:
time: 209 us; the launch traced here: 208 us
  Pallas kernels  201 us (96%)
  local copies, waits for them, and re-layouts  4.97 us (2%)
    pallas_call x1, Pallas kernels, body(): pl.pallas_call(functools.partial(layer_kernel, (n_ep, n_tp, tok, width, s...  201 us
    unnamed x5, local copies, waits for them, and re-layouts  4.89 us

commit v1 on v0

--- a/solution.py
+++ b/solution.py
@@ -29,18 +29,20 @@
     shape,
     xa_hbm, ga_ref, wq_hbm, wk_hbm, wf_hbm, wc_hbm, wg_hbm, shift_ref, fade_ref, first_ref,
     hgain_ref, wr_hbm,
-    x_hbm, gain_ref, meta_ref, wv_hbm, wu_hbm, wd_hbm, jv_hbm, ju_hbm, jd_hbm,
+    x_hbm, gain_ref, picks_ref, mixing_ref, wv_hbm, wu_hbm, wd_hbm, jv_hbm, ju_hbm, jd_hbm,
     mix_out, moe_out,
-    xa, na, wa, pj, att, qg, state, sent, heard, pt,
+    xa, na, wa, pj, att, qg, state, sent, heard, pt, blocks, fades,
     x_ref, wv, wu, wd, jv, ju, jd,
     gm, metas, onehot, weigh, tx, rx, hid, ry, shid, fx,
+    td, rd, rz, xr, xs, zs, fz,
     wsem, ags, agr, ms, mr, dts, drs, dls, rts, rrs, rls, fs, fr,
-    aas, aar, ss, sr, hs, hr,
+    aas, aar, ss, sr, hs, hr, nds, ndr, nxs, nxr, ros, ror, rcs, rcr, rzs, rzr, fzs, fzr, nls, hts, hrs, hls, hfs, hfr,
 ):
     n_ep, n_tp, tok, width, slots, ffe, seg, kw, vw = shape
     per = n_tp * 2 * slots
     rows = n_ep * per
     wc = width // CHUNKS
+    sub = wc // n_tp
     part_rows = 512
     heads = vw // 128
     segrows = seg * n_tp
@@ -87,8 +89,8 @@
     for c in range(CHUNKS):
         gm[c, mine, :] = normed[:, c * wc : (c + 1) * wc]
 
-    meta = meta_ref[...]
-    tall = jnp.concatenate([meta, jnp.zeros((tok - 8, tok), F32)], axis=0).T
+    meta = jnp.concatenate([picks_ref[...].astype(F32), mixing_ref[...]], axis=0)
+    tall = jnp.concatenate([meta, jnp.zeros((tok - 4, tok), F32)], axis=0).T
     before = lax.broadcasted_iota(jnp.int32, (tok, tok), 0) < lax.broadcasted_iota(
         jnp.int32, (tok, tok), 1
     )
@@ -112,14 +114,15 @@
 
     my_meta = metas.at[at(tp * 8, 8)]
     sends = []
-
-    def send_tp(src, dst, ssem, rsem, to):
+    gathers = []
+
+    def send_tp(src, dst, ssem, rsem, to, keep=None):
         copy = pltpu.make_async_remote_copy(
             src_ref=src, dst_ref=dst, send_sem=ssem, recv_sem=rsem,
             device_id={"tp": to}, device_id_type=MESH,
         )
         copy.start()
-        sends.append(copy)
+        (sends if keep is None else keep).append(copy)
 
     def arrived(ref, sem):
         pltpu.make_async_copy(ref, ref, sem).wait()
@@ -132,10 +135,13 @@
             return gm.at[c, at(who * tok, tok)]
         return gm.at[c, at(who * tok + half * (tok // 2), tok // 2)]
 
-    for c in range(CHUNKS):
+    def own_chunk(c):
         own = block(c, tp)
-        send_tp(own, own, ags.at[c, 0], agr.at[c, 0], right)
-        send_tp(own, own, ags.at[c, 1], agr.at[c, 1], left)
+        send_tp(own, own, ags.at[c, 0], agr.at[c, 0], right, gathers)
+        send_tp(own, own, ags.at[c, 1], agr.at[c, 1], left, gathers)
+
+    own_chunk(0)
+    own_chunk(1)
 
     loads[1].wait()
     for i in range(4):
@@ -150,30 +156,31 @@
         send_tp(own, own, aas.at[0, i], aar.at[0, i], right)
         send_tp(own, own, aas.at[1, i], aar.at[1, i], left)
 
-    for step in range(1, n_tp):
-        arrived(metas.at[at(lax.rem(tp + n_tp - step, n_tp) * 8, 8)], mr.at[step])
-
-    def table(t, carry):
-        r0 = pl.multiple_of(t * 256, 256)
-        ids = lax.broadcasted_iota(jnp.int32, (256, tok), 0) + r0
-        for m in range(n_tp):
-            spot = metas[8 * m : 8 * m + 2, :].astype(jnp.int32)
-            hit = (ids == spot[0:1]) | (ids == spot[1:2])
-            onehot[pl.ds(r0, 256), m * tok : (m + 1) * tok] = jnp.where(hit, 1.0, 0.0).astype(BF16)
-        return carry
-
-    lax.fori_loop(0, rows // 256, table, 0)
+    def build_tables():
+        for step in range(1, n_tp):
+            arrived(metas.at[at(lax.rem(tp + n_tp - step, n_tp) * 8, 8)], mr.at[step])
+
+        def table(t, carry):
+            r0 = pl.multiple_of(t * 256, 256)
+            ids = lax.broadcasted_iota(jnp.int32, (256, tok), 0) + r0
+            for m in range(n_tp):
+                spot = metas[8 * m : 8 * m + 2, :].astype(jnp.int32)
+                hit = (ids == spot[0:1]) | (ids == spot[1:2])
+                onehot[pl.ds(r0, 256), m * tok : (m + 1) * tok] = jnp.where(hit, 1.0, 0.0).astype(BF16)
+            return carry
+
+        lax.fori_loop(0, rows // 256, table, 0)
 
     def local_rows(c, src, dst, sem):
         own = at(ep * per, per)
-        return pltpu.make_async_copy(src.at[c, own], dst.at[c, own], sem.at[c])
+        return pltpu.make_async_copy(src.at[c, own], dst.at[c - 1 if dst is ry else c, own], sem.at[c])
 
     def spread(c, src, dst, ssem, rsem):
         def one(i, carry):
             to = peer(i)
             pltpu.make_async_remote_copy(
                 src_ref=src.at[c, at(to * per, per)],
-                dst_ref=dst.at[c, at(ep * per, per)],
+                dst_ref=dst.at[c - 1 if dst is ry else c, at(ep * per, per)],
                 send_sem=ssem.at[c], recv_sem=rsem.at[c],
                 device_id={"ep": to}, device_id_type=MESH,
             ).start()
@@ -182,8 +189,30 @@
         lax.fori_loop(1, n_ep, one, 0)
         local_rows(c, src, dst, dls if src is tx and dst is rx else rls).start()
 
+    def narrow_own(src, dst, k):
+        own = at(ep * per, per)
+        return pltpu.make_async_copy(src.at[own], dst.at[own], nls.at[k])
+
+    def spread_narrow(src, dst, ssem, rsem, k):
+        def one(i, carry):
+            to = peer(i)
+            pltpu.make_async_remote_copy(
+                src_ref=src.at[at(to * per, per)],
+                dst_ref=dst.at[at(ep * per, per)],
+                send_sem=ssem.at[0], recv_sem=rsem.at[0],
+                device_id={"ep": to}, device_id_type=MESH,
+            ).start()
+            return carry
+
+        lax.fori_loop(1, n_ep, one, 0)
+        narrow_own(src, dst, k).start()
+
+    def narrow_done(ref, sem):
+        some = ref.at[pl.ds(0, rows - per)]
+        pltpu.make_async_copy(some, some, sem.at[0]).wait()
+
     def all_but_one(ref, c, sem):
-        some = ref.at[c, pl.ds(0, rows - per)]
+        some = ref.at[c - 1 if ref is ry else c, pl.ds(0, rows - per)]
         pltpu.make_async_copy(some, some, sem.at[c]).wait()
 
     def project(who):
@@ -196,77 +225,10 @@
 
         lax.fori_loop(0, (3 * kw + 2 * vw) // 256, one, 0)
 
-    for c in range(CHUNKS):
-        arrived(block(c, left), agr.at[c, 0])
-        fwd = block(c, left, 0)
-        send_tp(fwd, fwd, ags.at[c, 2], agr.at[c, 2], right)
-        arrived(block(c, right), agr.at[c, 1])
-        fwd = block(c, right, 1)
-        send_tp(fwd, fwd, ags.at[c, 3], agr.at[c, 3], left)
-        attention_send(c)
-        arrived(block(c, across, 0), agr.at[c, 2])
-        arrived(block(c, across, 1), agr.at[c, 3])
-
-        def build(t, carry, c=c):
-            r = at(t * part_rows, part_rows)
-            tx[c, r, :] = jnp.dot(onehot[r, :], gm[c], preferred_element_type=F32).astype(BF16)
-            return carry
-
-        lax.fori_loop(0, rows // part_rows, build, 0)
-        spread(c, tx, rx, dts, drs)
-        if c == 0:
-            for copy in loads[2:7]:
-                copy.wait()
-            project(tp)
-
-    for i in range(4):
-        arrived(ablock(left, i), aar.at[0, i])
-        if i < 2:
-            fwd = ablock(left, i)
-            send_tp(fwd, fwd, aas.at[2, i], aar.at[2, i], right)
-        arrived(ablock(right, i), aar.at[1, i])
-        if i >= 2:
-            fwd = ablock(right, i)
-            send_tp(fwd, fwd, aas.at[2, i], aar.at[2, i], left)
-    project(left)
-    project(right)
-
-    loads[7].wait()
-    loads[8].wait()
-
-    def shared(t, carry):
-        r = at(t * tok, tok)
-        g = jnp.zeros((tok, jv.shape[1]), F32)
-        u = jnp.zeros((tok, jv.shape[1]), F32)
-        for c in range(CHUNKS):
-            xs = gm[c, r, :]
-            g = g + jnp.dot(xs, jv[c * wc : (c + 1) * wc, :], preferred_element_type=F32)
-            u = u + jnp.dot(xs, ju[c * wc : (c + 1) * wc, :], preferred_element_type=F32)
-        shid[r, :] = (jax.nn.silu(g) * u).astype(BF16)
-        return carry
-
-    lax.fori_loop(0, n_tp, shared, 0)
-
-    def weights(m, carry):
-        both = jnp.concatenate([metas[at(8 * m, 8), :], jnp.zeros((tok - 8, tok), F32)], axis=0).T
-        spot = both[:, 0:2].astype(jnp.int32)
-        for c in range(rows // 256):
-            ids = lax.broadcasted_iota(jnp.int32, (tok, 256), 1) + c * 256
-            w = jnp.where(ids == spot[:, 0:1], both[:, 2:3], 0.0) + jnp.where(
-                ids == spot[:, 1:2], both[:, 3:4], 0.0
-            )
-            weigh[at(m * tok, tok), c * 256 : (c + 1) * 256] = w.astype(BF16)
-        return carry
-
-    lax.fori_loop(0, n_tp, weights, 0)
-
-    for i in range(4):
-        arrived(ablock(across, i), aar.at[2, i])
-    project(across)
-    late_load = pltpu.make_async_copy(wr_hbm, wa, wsem.at[13])
-    late_load.start()
-
-    state[...] = jnp.zeros_like(state)
+    def after(first, second):
+        return first[0] * second[0], second[0] * first[1] + second[1]
+
+    neutral = (jnp.ones((kw, 128), F32), jnp.zeros((kw, 128), F32))
 
     def iota(dims, axis):
         return lax.broadcasted_iota(jnp.int32, dims, axis)
@@ -285,7 +247,7 @@
         k = pj[r, kw : 2 * kw].astype(F32)
         z = pj[r, 2 * kw : 3 * kw].astype(F32) + shift_ref[...]
         v = pj[r, 3 * kw : 3 * kw + vw]
-        extra = fade_ref[r, :]
+        extra = fades[r, :]
         add = extra[:, 0:1]
         for h in range(1, heads):
             add = jnp.where(head_of == h, extra[:, h : h + 1], add)
@@ -314,17 +276,106 @@
         state[...] = jnp.concatenate([fade] * heads, axis=1) * held + grown * vmask
         return past + total, past_tall + tall_total
 
-    _, whole = lax.fori_loop(
-        0, segrows // SPAN, span, (jnp.zeros((1, kw), F32), jnp.zeros((kw, 128), F32))
-    )
-    own_fade = jnp.exp(whole)
-    own_state = jnp.concatenate(
-        [state[64 * h : 64 * h + 64, 128 * h : 128 * h + 128] for h in range(heads)], axis=0
-    )
+    def spans(who):
+        state[...] = jnp.zeros_like(state)
+        first = who * (seg // SPAN)
+        _, tall_log = lax.fori_loop(
+            0, seg // SPAN, lambda n, carry: span(first + n, carry),
+            (jnp.zeros((1, kw), F32), jnp.zeros((kw, 128), F32)),
+        )
+        blocks[who, 0] = jnp.exp(tall_log)
+        for h in range(heads):
+            blocks[who, 1, 64 * h : 64 * h + 64, :] = state[64 * h : 64 * h + 64, 128 * h : 128 * h + 128]
+
+    def forward(c):
+        arrived(block(c, left), agr.at[c, 0])
+        fwd = block(c, left, 0)
+        send_tp(fwd, fwd, ags.at[c, 2], agr.at[c, 2], right, gathers)
+        arrived(block(c, right), agr.at[c, 1])
+        fwd = block(c, right, 1)
+        send_tp(fwd, fwd, ags.at[c, 3], agr.at[c, 3], left, gathers)
+
+    def dispatch(c):
+        arrived(block(c, across, 0), agr.at[c, 2])
+        arrived(block(c, across, 1), agr.at[c, 3])
+
+        def build(t, carry):
+            r = at(t * part_rows, part_rows)
+            tx[c, r, :] = jnp.dot(onehot[r, :], gm[c], preferred_element_type=F32).astype(BF16)
+            return carry
+
+        def narrow(t, carry):
+            r = at(t * part_rows, part_rows)
+            td[r, :] = jnp.dot(
+                onehot[r, :], gm[0, :, at(tp * sub, sub)], preferred_element_type=F32
+            ).astype(BF16)
+            return carry
+
+        if c == 0:
+            lax.fori_loop(0, rows // part_rows, narrow, 0)
+            spread_narrow(td, rd, nds, ndr, 0)
+        else:
+            lax.fori_loop(0, rows // part_rows, build, 0)
+            spread(c, tx, rx, dts, drs)
+
+    forward(0)
+    build_tables()
+    forward(1)
+    own_chunk(2)
+    attention_send(0)
+    dispatch(0)
+    dispatch(1)
+    forward(2)
+    attention_send(1)
+    own_chunk(3)
+    attention_send(2)
+    attention_send(3)
+    for copy in loads[2:7]:
+        copy.wait()
+    project(tp)
+    dispatch(2)
+    for m in range(n_tp * seg // 128):
+        wide = jnp.concatenate([fade_ref[:, 128 * m : 128 * m + 128], jnp.zeros((124, 128), F32)], axis=0)
+        fades[128 * m : 128 * m + 128, :] = wide.T
+    spans(tp)
+    forward(3)
+    for i in range(4):
+        arrived(ablock(left, i), aar.at[0, i])
+        if i < 2:
+            fwd = ablock(left, i)
+            send_tp(fwd, fwd, aas.at[2, i], aar.at[2, i], right)
+        arrived(ablock(right, i), aar.at[1, i])
+        if i >= 2:
+            fwd = ablock(right, i)
+            send_tp(fwd, fwd, aas.at[2, i], aar.at[2, i], left)
+    narrow_own(td, rd, 0).wait()
+    narrow_done(rd, ndr)
+    my_slice = rx.at[0, :, at(tp * sub, sub)]
+    for step in range(1, n_tp):
+        send_tp(rd, my_slice, nxs.at[step], nxr.at[step], lax.rem(tp + step, n_tp))
+    keep = pltpu.make_async_copy(rd, my_slice, nls.at[1])
+    keep.start()
+    dispatch(3)
+    project(left)
+    project(right)
+    spans(left)
+    spans(right)
+    for i in range(4):
+        arrived(ablock(across, i), aar.at[2, i])
+    project(across)
+    spans(across)
+    late_load = pltpu.make_async_copy(wr_hbm, wa, wsem.at[13])
+    late_load.start()
+    whole = neutral
+    for m in range(n_tp):
+        whole = after(whole, (blocks[m, 0], blocks[m, 1]))
+    own_fade, own_state = whole
 
     def put(level, fade, held):
-        sent[level, 0] = fade.astype(BF16)
-        sent[level, 1] = held.astype(BF16)
+        rows_of = [fade[128 * i : 128 * i + 128].T[0:8] for i in range(kw // 128)]
+        flat = jnp.concatenate([rows_of[0][0:1], rows_of[1][0:1], jnp.zeros((14, 128), F32)], axis=0)
+        sent[level, 0:kw] = held.astype(BF16)
+        sent[level, kw : kw + 16] = flat.astype(BF16)
 
     def share(level, slot, to):
         pltpu.make_async_remote_copy(
@@ -336,16 +387,18 @@
         arrived(heard.at[slot], sr.at[slot])
         pltpu.make_async_copy(sent.at[level], sent.at[level], ss.at[slot]).wait()
 
-    def after(first, second):
-        return first[0] * second[0], second[0] * first[1] + second[1]
-
     def pick(flag, pair, other):
         return tuple(jnp.where(flag, a, b) for a, b in zip(pair, other))
 
-    neutral = (jnp.ones((kw, 128), F32), jnp.zeros((kw, 128), F32))
-
     def load_pair(slot):
-        return heard[slot, 0].astype(F32), heard[slot, 1].astype(F32)
+        return unpack(heard[slot])
+
+    def unpack(packed):
+        flat = packed[kw : kw + 16].astype(F32)
+        fade = jnp.concatenate(
+            [jnp.broadcast_to(flat[i : i + 1], (128, 128)).T for i in range(kw // 128)], axis=0
+        )
+        return fade, packed[0:kw].astype(F32)
 
     def ring_fold(base, place, me):
         prefix, everything = neutral, neutral
@@ -364,7 +417,7 @@
     def level_one():
         hear(0, 0)
         mate = load_pair(0)
-        me = (sent[0, 0].astype(F32), sent[0, 1].astype(F32))
+        me = unpack(sent[0])
         low, high = pick(core == 0, me, mate), pick(core == 0, mate, me)
         chip = after(low, high)
         put(1, *chip)
@@ -387,14 +440,30 @@
         return ring_fold(4, zz, column)[0]
 
     in_chip, chip = level_one()
+    loads[7].wait()
+    loads[8].wait()
+
+    def shared(t, carry):
+        r = at(t * tok, tok)
+        g = jnp.zeros((tok, jv.shape[1]), F32)
+        u = jnp.zeros((tok, jv.shape[1]), F32)
+        for c in range(CHUNKS):
+            xs = gm[c, r, :]
+            g = g + jnp.dot(xs, jv[c * wc : (c + 1) * wc, :], preferred_element_type=F32)
+            u = u + jnp.dot(xs, ju[c * wc : (c + 1) * wc, :], preferred_element_type=F32)
+        shid[r, :] = (jax.nn.silu(g) * u).astype(BF16)
+        return carry
+
+    lax.fori_loop(0, n_tp, shared, 0)
 
     for copy in loads[9:11]:
         copy.wait()
-    for c in range(CHUNKS):
+    keep.wait()
+    for step in range(1, n_tp):
+        arrived(rx.at[0, :, at(lax.rem(tp + n_tp - step, n_tp) * sub, sub)], nxr.at[step])
+    for c in range(1, CHUNKS):
         local_rows(c, tx, rx, dls).wait()
         all_but_one(rx, c, drs)
-
-    in_column, column = level_two(chip)
 
     def expert(t, carry):
         r = at(t * part_rows, part_rows)
@@ -412,29 +481,67 @@
         return carry
 
     lax.fori_loop(0, rows // part_rows, expert, 0)
-    in_slice = level_three(column)
-    earlier = after(after(in_slice, in_column), in_chip)
+    in_column, column = level_two(chip)
 
     loads[11].wait()
-    for c in range(CHUNKS):
-        all_but_one(tx, c, dts)
-
-        def down(t, carry, c=c):
+    loads[12].wait()
+    narrow_done(td, nds)
+    for copy in gathers:
+        copy.wait_send()
+
+    def down(c):
+        def one(t, carry):
             r = at(t * part_rows, part_rows)
             tx[c, r, :] = jnp.dot(
                 hid[r, :], wd[:, c * wc : (c + 1) * wc], preferred_element_type=F32
             ).astype(BF16)
             return carry
 
-        lax.fori_loop(0, rows // part_rows, down, 0)
-        spread(c, tx, ry, rts, rrs)
+        lax.fori_loop(0, rows // part_rows, one, 0)
+
+    all_but_one(tx, 1, dts)
+    down(1)
+    spread(1, tx, ry, rts, rrs)
+    down(0)
+    gm[0, :, :] = jnp.dot(shid[...], jd[:, 0:wc], preferred_element_type=F32).astype(BF16)
+    for step in range(1, n_tp):
+        to = lax.rem(tp + step, n_tp)
+        cols = at(to * sub, sub)
+        send_tp(tx.at[0, :, cols], xr.at[step - 1], ros.at[step], ror.at[step], to)
+        send_tp(gm.at[0, :, cols], xs.at[step - 1], rcs.at[step], rcr.at[step], to)
+    all_but_one(tx, 2, dts)
+    down(2)
+    spread(2, tx, ry, rts, rrs)
+    all_but_one(tx, 3, dts)
+    down(3)
+
+    def weights(m, carry):
+        both = jnp.concatenate([metas[at(8 * m, 8), :], jnp.zeros((tok - 8, tok), F32)], axis=0).T
+        spot = both[:, 0:2].astype(jnp.int32)
+        for c in range(rows // 256):
+            ids = lax.broadcasted_iota(jnp.int32, (tok, 256), 1) + c * 256
+            w = jnp.where(ids == spot[:, 0:1], both[:, 2:3], 0.0) + jnp.where(
+                ids == spot[:, 1:2], both[:, 3:4], 0.0
+            )
+            weigh[at(m * tok, tok), c * 256 : (c + 1) * 256] = w.astype(BF16)
+        return carry
+
+    lax.fori_loop(0, n_tp, weights, 0)
+
+    in_slice = level_three(column)
+    earlier = after(after(in_slice, in_column), in_chip)
 
     entering = earlier[1] + earlier[0] * first_ref[...]
-    wide_entry = jnp.concatenate([entering.astype(BF16)] * heads, axis=1) * vmask16
+    for m in range(n_tp):
+        fade, held = blocks[m, 0], blocks[m, 1]
+        blocks[m, 1] = entering
+        entering = fade * entering + held
+
     for step in range(n_tp):
         who = lax.rem(tp + step + 1, n_tp)
-
-        def finish(i, carry, who=who):
+        wide_entry = jnp.concatenate([blocks[who, 1].astype(BF16)] * heads, axis=1) * vmask16
+
+        def finish(i, carry, who=who, wide_entry=wide_entry):
             r = at(who * seg + i * 128, 128)
             full = att[r, :] + jnp.dot(qg[r, :], wide_entry, preferred_element_type=F32)
             for h in range(heads):
@@ -449,6 +556,75 @@
         if step < n_tp - 1:
             send_tp(pj.at[at(who * seg, seg), 0:vw], pt.at[step], hs.at[step], hr.at[step], who)
 
+    last = []
+
+    def collect(c):
+        local_rows(c, tx, ry, rls).wait()
+        all_but_one(ry, c, rrs)
+
+        def combine(m, carry, c=c):
+            r = at(m * 256, 256)
+            got = jnp.dot(weigh[r, :], ry[c - 1], preferred_element_type=F32)
+            got = got + jnp.dot(shid[r, :], jd[:, c * wc : (c + 1) * wc], preferred_element_type=F32)
+            gm[c, r, :] = got.astype(BF16)
+            return carry
+
+        lax.fori_loop(0, n_tp * tok // 256, combine, 0)
+        for step in range(1, n_tp):
+            to = lax.rem(tp + step, n_tp)
+            copy = pltpu.make_async_remote_copy(
+                src_ref=gm.at[c, at(to * tok, tok)],
+                dst_ref=fx.at[c - 1, step - 1],
+                send_sem=fs.at[c, step], recv_sem=fr.at[c, step],
+                device_id={"tp": to}, device_id_type=MESH,
+            )
+            copy.start()
+            last.append(copy)
+
+    collect(1)
+    for step in range(1, n_tp):
+        arrived(xr.at[step - 1], ror.at[step])
+        arrived(xs.at[step - 1], rcr.at[step])
+
+    def slices(t, carry):
+        r = at(t * 256, 256)
+        got = tx[0, r, at(tp * sub, sub)].astype(F32)
+        for step in range(n_tp - 1):
+            got = got + xr[step, r, :].astype(F32)
+        td[r, :] = got.astype(BF16)
+        return carry
+
+    lax.fori_loop(0, rows // 256, slices, 0)
+    spread_narrow(td, rz, rzs, rzr, 2)
+    hc = wc // 2
+
+    def spread_half(k):
+        cols = pl.ds(k * hc, hc)
+
+        def one(i, carry):
+            to = peer(i)
+            pltpu.make_async_remote_copy(
+                src_ref=tx.at[3, at(to * per, per), cols],
+                dst_ref=ry.at[2, at(ep * per, per), cols],
+                send_sem=hts.at[k], recv_sem=hrs.at[k],
+                device_id={"ep": to}, device_id_type=MESH,
+            ).start()
+            return carry
+
+        lax.fori_loop(1, n_ep, one, 0)
+        half_own(k).start()
+
+    def half_own(k):
+        own, cols = at(ep * per, per), pl.ds(k * hc, hc)
+        return pltpu.make_async_copy(tx.at[3, own, cols], ry.at[2, own, cols], hls.at[k])
+
+    def half_done(ref, k, sem):
+        some = ref.at[pl.ds(0, rows - per), pl.ds(k * hc, hc)]
+        pltpu.make_async_copy(some, some, sem.at[k]).wait()
+
+    spread_half(0)
+    spread_half(1)
+    collect(2)
     late_load.wait()
     from_self = pj[at(tp * seg, seg), 0:vw]
     for step in range(n_tp - 1):
@@ -465,41 +641,78 @@
 
     lax.fori_loop(0, width // 512, result, 0)
 
-    for copy in sends:
-        copy.wait_send()
-
-    loads[12].wait()
-    last = []
-    for c in range(CHUNKS):
-        local_rows(c, tx, ry, rls).wait()
-        all_but_one(ry, c, rrs)
-
-        def combine(m, carry, c=c):
+    narrow_own(td, rz, 2).wait()
+    narrow_done(rz, rzr)
+    for m in range(n_tp):
+        r = slice(m * tok, (m + 1) * tok)
+        got = jnp.dot(weigh[r, :], rz[...], preferred_element_type=F32)
+        got = got + gm[0, r, at(tp * sub, sub)].astype(F32)
+        for step in range(n_tp - 1):
+            got = got + xs[step, r, :].astype(F32)
+        zs[r, :] = got.astype(BF16)
+    final = []
+    for step in range(1, n_tp):
+        to = lax.rem(tp + step, n_tp)
+        copy = pltpu.make_async_remote_copy(
+            src_ref=zs.at[at(to * tok, tok)], dst_ref=fz.at[step - 1],
+            send_sem=fzs.at[step], recv_sem=fzr.at[step],
+            device_id={"tp": to}, device_id_type=MESH,
+        )
+        copy.start()
+        final.append(copy)
+
+    halves = []
+
+    def collect_half(k):
+        half_own(k).wait()
+        half_done(ry.at[2], k, hrs)
+
+        def combine(m, carry):
             r = at(m * 256, 256)
-            got = jnp.dot(weigh[r, :], ry[c], preferred_element_type=F32)
-            got = got + jnp.dot(shid[r, :], jd[:, c * wc : (c + 1) * wc], preferred_element_type=F32)
-            gm[c, r, :] = got.astype(BF16)
+            got = jnp.dot(weigh[r, :], ry[2, :, k * hc : (k + 1) * hc], preferred_element_type=F32)
+            got = got + jnp.dot(
+                shid[r, :], jd[:, 3 * wc + k * hc : 3 * wc + (k + 1) * hc], preferred_element_type=F32
+            )
+            gm[3, r, k * hc : (k + 1) * hc] = got.astype(BF16)
             return carry
 
         lax.fori_loop(0, n_tp * tok // 256, combine, 0)
         for step in range(1, n_tp):
             to = lax.rem(tp + step, n_tp)
             copy = pltpu.make_async_remote_copy(
-                src_ref=gm.at[c, at(to * tok, tok)],
-                dst_ref=fx.at[c, step - 1],
-                send_sem=fs.at[c, step], recv_sem=fr.at[c, step],
+                src_ref=gm.at[3, at(to * tok, tok), pl.ds(k * hc, hc)],
+                dst_ref=fx.at[2, step - 1, :, pl.ds(k * hc, hc)],
+                send_sem=hfs.at[k, step], recv_sem=hfr.at[k, step],
                 device_id={"tp": to}, device_id_type=MESH,
             )
             copy.start()
-            last.append(copy)
-
-    for c in range(CHUNKS):
+            halves.append(copy)
+
+    collect_half(0)
+    for c in range(1, CHUNKS - 1):
         total = gm[c, mine, :].astype(F32)
         for step in range(1, n_tp):
-            last[c * (n_tp - 1) + step - 1].wait()
-            total = total + fx[c, step - 1].astype(F32)
+            last[(c - 1) * (n_tp - 1) + step - 1].wait()
+            total = total + fx[c - 1, step - 1].astype(F32)
         moe_out[:, c * wc : (c + 1) * wc] = total.astype(BF16)
         all_but_one(tx, c, rts)
+    moe_out[:, at(tp * sub, sub)] = zs[mine, :]
+    narrow_done(td, rzs)
+    for step in range(1, n_tp):
+        final[step - 1].wait()
+        moe_out[:, at(lax.rem(tp + n_tp - step, n_tp) * sub, sub)] = fz[step - 1]
+    collect_half(1)
+    for copy in sends:
+        copy.wait_send()
+
+    for k in range(2):
+        cols = slice(k * hc, (k + 1) * hc)
+        total = gm[3, mine, cols].astype(F32)
+        for step in range(1, n_tp):
+            halves[k * (n_tp - 1) + step - 1].wait()
+            total = total + fx[2, step - 1, :, cols].astype(F32)
+        moe_out[:, 3 * wc + k * hc : 3 * wc + (k + 1) * hc] = total.astype(BF16)
+        half_done(tx.at[3], k, hts)
 
 
 def body(
@@ -514,7 +727,7 @@
     slots = 3 * tok * 2 // (2 * n_ep * local)
     rows = n_ep * n_tp * 2 * slots
     wc = width // CHUNKS
-    meta = jnp.concatenate([picked.T.astype(F32), mixing.T, jnp.zeros((4, tok), F32)], axis=0)
+    sub = wc // n_tp
     hbm = pl.BlockSpec(memory_space=pl.ANY)
     vmem = pl.BlockSpec(memory_space=pltpu.VMEM)
     dma = pltpu.SemaphoreType.DMA
@@ -525,7 +738,7 @@
             jax.ShapeDtypeStruct((seg, width), BF16),
             jax.ShapeDtypeStruct((tok, width), BF16),
         ),
-        in_specs=[hbm, vmem] + [hbm] * 5 + [vmem] * 4 + [hbm] + [hbm, vmem, vmem] + [hbm] * 6,
+        in_specs=[hbm, vmem] + [hbm] * 5 + [vmem] * 4 + [hbm] + [hbm, vmem, vmem, vmem] + [hbm] * 6,
         out_specs=(vmem, vmem),
         scratch_shapes=[
             V((seg, width), BF16),
@@ -535,9 +748,11 @@
             V((seg * n_tp, vw), F32),
             V((seg * n_tp, kw), BF16),
             V((kw, vw), F32),
-            V((3, 2, kw, 128), BF16),
-            V((7, 2, kw, 128), BF16),
+            V((3, kw + 16, 128), BF16),
+            V((7, kw + 16, 128), BF16),
             V((n_tp - 1, seg, vw), BF16),
+            V((n_tp, 2, kw, 128), F32),
+            V((seg * n_tp, 128), F32),
             V((tok, width), BF16), V(wv.shape, BF16), V(wu.shape, BF16), V((2 * ffe, width), BF16),
             V(jv.shape, BF16), V(ju.shape, BF16), V(jd.shape, BF16),
             V((CHUNKS, n_tp * tok, wc), BF16),
@@ -547,23 +762,29 @@
             V((CHUNKS, rows, wc), BF16),
             V((CHUNKS, rows, wc), BF16),
             V((rows, 2 * ffe), BF16),
-            V((CHUNKS, rows, wc), BF16),
+            V((CHUNKS - 1, rows, wc), BF16),
             V((n_tp * tok, jv.shape[1]), BF16),
-            V((CHUNKS, n_tp - 1, tok, wc), BF16),
+            V((CHUNKS - 1, n_tp - 1, tok, wc), BF16),
+            V((rows, sub), BF16), V((rows, sub), BF16), V((rows, sub), BF16),
+            V((n_tp - 1, rows, sub), BF16), V((n_tp - 1, n_tp * tok, sub), BF16),
+            V((n_tp * tok, sub), BF16), V((n_tp - 1, tok, sub), BF16),
             dma((14,)), dma((CHUNKS, 4)), dma((CHUNKS, 4)), dma((n_tp,)), dma((n_tp,)),
             dma((CHUNKS,)), dma((CHUNKS,)), dma((CHUNKS,)),
             dma((CHUNKS,)), dma((CHUNKS,)), dma((CHUNKS,)),
             dma((CHUNKS, n_tp)), dma((CHUNKS, n_tp)),
             dma((3, 4)), dma((3, 4)), dma((7,)), dma((7,)), dma((n_tp,)), dma((n_tp,)),
+            dma((1,)), dma((1,)), dma((n_tp,)), dma((n_tp,)), dma((n_tp,)), dma((n_tp,)), dma((n_tp,)), dma((n_tp,)),
+            dma((1,)), dma((1,)), dma((n_tp,)), dma((n_tp,)), dma((3,)),
+            dma((2,)), dma((2,)), dma((2,)), dma((2, n_tp)), dma((2, n_tp)),
         ],
         compiler_params=pltpu.CompilerParams(
             collective_id=0, has_side_effects=True, vmem_limit_bytes=67043328
         ),
         name="layer",
     )(
-        xa, ga.reshape(1, -1), wq, wk, wf, wc_, wg, shift.reshape(1, -1), fade, first,
+        xa, ga.reshape(1, -1), wq, wk, wf, wc_, wg, shift.reshape(1, -1), fade.T, first,
         hgain.reshape(1, -1), wr,
-        x, gain.reshape(1, -1), meta, wv, wu, wd.reshape(2 * ffe, width), jv, ju, jd,
+        x, gain.reshape(1, -1), picked.T, mixing.T, wv, wu, wd.reshape(2 * ffe, width), jv, ju, jd,
     )
 
 

time: 209 us -> 175 us (0.84)
  Pallas kernels: 201 us -> 171 us
    pallas_call x1, Pallas kernels: 201 us -> 171 us  [body(): pl.pallas_call(functools.partial(layer_kernel, (n_ep, n_tp, tok, width, s...]
    unnamed x5 -> x4, local copies, waits for them, and re-layouts: 4.89 us -> 3.16 us
where the time goes in v1:
time: 175 us
  Pallas kernels  171 us (98%)
  local copies, waits for them, and re-layouts  3.16 us (2%)
    pallas_call x1, Pallas kernels, body(): pl.pallas_call(functools.partial(layer_kernel, (n_ep, n_tp, tok, width, s...  171 us

profile of v1, /device:TPU:0, one launch (start us, length us, event | category | flops | bytes accessed | tf_op | source)
XLA Modules:
  0.0 174.9 jit_solution(4461914230185285186)
XLA Ops:
  0.6 171.1 %layer.1 = (bf16[256,2048]{1,0:T(8,128)(2,1)}, bf16[128,2048]{1,0:T(8,128)(2,1)}) custom-call(bf16[256,2048]{1,0:T(8,128)(2,1)} %xa_hbm.1, f32[1,2048]{1,0:T(1,128)} %bitcast.10, bf16[2048,256]{1,0:T(8,128)(2,1)} %wq_hbm.1, bf16[2048,256]{1,0:T(8,128)(2,1)} %wk_hbm.1, bf16[2048,256]{1,0:T(8,128)(2,1)} %wf_hbm.1, bf16[2048,512]{1,0:T(8,128)(2,1)} %wc_hbm.1, ...), custom_call_target="tpu_custom_call" | custom-call | tf_op jit(solution)/shard_map/layer/pallas_call | solution.py:735
  171.7 0.0 copy-start
  171.8 2.4 %copy.26 = bf16[256,2048]{1,0:T(8,128)(2,1)} copy(bf16[256,2048]{1,0:T(8,128)(2,1)} %get-tuple-element.4) | data formatting | bytes 2097152
  174.1 0.0 copy-done
  174.1 0.8 copy.27
Async XLA Ops:
  171.7 2.4 %copy-start = (bf16[128,2048]{1,0:T(8,128)(2,1)S(1)}, bf16[128,2048]{1,0:T(8,128)(2,1)}, u32[]{:S(2)}) copy-start(bf16[128,2048]{1,0:T(8,128)(2,1)} %get-tuple-element.5) | copy-start | bytes 1572868

commit v2 on v1

--- a/solution.py
+++ b/solution.py
@@ -34,16 +34,16 @@
     xa, na, wa, pj, att, qg, state, sent, heard, pt, blocks, fades,
     x_ref, wv, wu, wd, jv, ju, jd,
     gm, metas, onehot, weigh, tx, rx, hid, ry, shid, fx,
-    td, rd, rz, xr, xs, zs, fz,
+    td, rd, rz, xr, xs, zs, fz, gs,
     wsem, ags, agr, ms, mr, dts, drs, dls, rts, rrs, rls, fs, fr,
-    aas, aar, ss, sr, hs, hr, nds, ndr, nxs, nxr, ros, ror, rcs, rcr, rzs, rzr, fzs, fzr, nls, hts, hrs, hls, hfs, hfr,
+    aas, aar, ss, sr, hs, hr, nds, ndr, nxs, nxr, ros, ror, rcs, rcr, rzs, rzr, fzs, fzr, nls, hts, hrs, hls, hfs, hfr, gss, gsr,
 ):
     n_ep, n_tp, tok, width, slots, ffe, seg, kw, vw = shape
     per = n_tp * 2 * slots
     rows = n_ep * per
     wc = width // CHUNKS
     sub = wc // n_tp
-    part_rows = 512
+    part_rows = rows
     heads = vw // 128
     segrows = seg * n_tp
     quarter = seg // 4
@@ -60,6 +60,16 @@
             + lax.rem(yy + lax.rem(i // 2, 4), 4) * 2
             + lax.rem(core + lax.rem(i, 2), 2)
         )
+
+    def partner(k):
+        return peer(lax.rem(k * 11, n_ep))
+
+    def place_there(k):
+        i = lax.rem(k * 11, n_ep)
+        back = (
+            lax.rem(4 - i // 8, 4) * 8 + lax.rem(4 - lax.rem(i // 2, 4), 4) * 2 + lax.rem(i, 2)
+        )
+        return lax.rem(back * 3, n_ep)
 
     pairs = [
         (x_hbm, x_ref), (xa_hbm, xa),
@@ -104,7 +114,7 @@
             hits = hits + jnp.where((tall_names[:, j : j + 1] == row) & before, 1.0, 0.0)
         rank = jnp.sum(hits, axis=0, keepdims=True)
         local = row // 2
-        base = (local * per + tp * 2 * slots + (row - 2 * local) * slots).astype(F32)
+        base = (local * per + (row - 2 * local) * (n_tp * slots) + tp * slots).astype(F32)
         spots.append(base + rank)
     metas[at(tp * 8, 8), :] = jnp.concatenate(
         [spots[0], spots[1], meta[2:4], jnp.zeros((4, tok), F32)], axis=0
@@ -140,8 +150,14 @@
         send_tp(own, own, ags.at[c, 0], agr.at[c, 0], right, gathers)
         send_tp(own, own, ags.at[c, 1], agr.at[c, 1], left, gathers)
 
-    own_chunk(0)
+    gs[mine, :] = gm[0, mine, at(tp * sub, sub)]
+    for step in range(1, n_tp):
+        to = lax.rem(tp + step, n_tp)
+        send_tp(
+            gm.at[0, mine, at(to * sub, sub)], gs.at[mine], gss.at[step], gsr.at[step], to, gathers
+        )
     own_chunk(1)
+    own_chunk(2)
 
     loads[1].wait()
     for i in range(4):
@@ -171,34 +187,47 @@
 
         lax.fori_loop(0, rows // 256, table, 0)
 
+    def ends(k, out):
+        to = partner(k)
+        if out:
+            return to, at(to * per, per), at(place_there(k) * per, per)
+        return to, at(k * per, per), at(ep * per, per)
+
     def local_rows(c, src, dst, sem):
-        own = at(ep * per, per)
-        return pltpu.make_async_copy(src.at[c, own], dst.at[c - 1 if dst is ry else c, own], sem.at[c])
+        out = dst is rx
+        own, there = at(ep * per, per), pl.ds(0, per)
+        return pltpu.make_async_copy(
+            src.at[c, own if out else there], dst.at[c if out else c - 1, there if out else own], sem.at[c]
+        )
 
     def spread(c, src, dst, ssem, rsem):
-        def one(i, carry):
-            to = peer(i)
+        out = dst is rx
+
+        def one(k, carry):
+            to, here, there = ends(k, out)
             pltpu.make_async_remote_copy(
-                src_ref=src.at[c, at(to * per, per)],
-                dst_ref=dst.at[c - 1 if dst is ry else c, at(ep * per, per)],
+                src_ref=src.at[c, here],
+                dst_ref=dst.at[c if out else c - 1, there],
                 send_sem=ssem.at[c], recv_sem=rsem.at[c],
                 device_id={"ep": to}, device_id_type=MESH,
             ).start()
             return carry
 
         lax.fori_loop(1, n_ep, one, 0)
-        local_rows(c, src, dst, dls if src is tx and dst is rx else rls).start()
+        local_rows(c, src, dst, dls if out else rls).start()
 
     def narrow_own(src, dst, k):
-        own = at(ep * per, per)
-        return pltpu.make_async_copy(src.at[own], dst.at[own], nls.at[k])
+        own, there = at(ep * per, per), pl.ds(0, per)
+        if dst is rd:
+            return pltpu.make_async_copy(src.at[own], dst.at[there], nls.at[k])
+        return pltpu.make_async_copy(src.at[there], dst.at[own], nls.at[k])
 
     def spread_narrow(src, dst, ssem, rsem, k):
         def one(i, carry):
-            to = peer(i)
+            to, here, there = ends(i, dst is rd)
             pltpu.make_async_remote_copy(
-                src_ref=src.at[at(to * per, per)],
-                dst_ref=dst.at[at(ep * per, per)],
+                src_ref=src.at[here],
+                dst_ref=dst.at[there],
                 send_sem=ssem.at[0], recv_sem=rsem.at[0],
                 device_id={"ep": to}, device_id_type=MESH,
             ).start()
@@ -218,12 +247,9 @@
     def project(who):
         r = at(who * seg, seg)
 
-        def one(n, carry):
-            cols = at(n * 256, 256)
+        for n in range((3 * kw + 2 * vw) // 256):
+            cols = slice(n * 256, (n + 1) * 256)
             pj[r, cols] = jnp.dot(na[r, :], wa[:, cols], preferred_element_type=F32).astype(BF16)
-            return carry
-
-        lax.fori_loop(0, (3 * kw + 2 * vw) // 256, one, 0)
 
     def after(first, second):
         return first[0] * second[0], second[0] * first[1] + second[1]
@@ -281,7 +307,7 @@
         first = who * (seg // SPAN)
         _, tall_log = lax.fori_loop(
             0, seg // SPAN, lambda n, carry: span(first + n, carry),
-            (jnp.zeros((1, kw), F32), jnp.zeros((kw, 128), F32)),
+            (jnp.zeros((1, kw), F32), jnp.zeros((kw, 128), F32)), unroll=2,
         )
         blocks[who, 0] = jnp.exp(tall_log)
         for h in range(heads):
@@ -295,9 +321,16 @@
         fwd = block(c, right, 1)
         send_tp(fwd, fwd, ags.at[c, 3], agr.at[c, 3], left, gathers)
 
-    def dispatch(c):
+    def far(c):
         arrived(block(c, across, 0), agr.at[c, 2])
         arrived(block(c, across, 1), agr.at[c, 3])
+
+    def dispatch(c):
+        if c == 0:
+            for step in range(1, n_tp):
+                arrived(gs.at[at(lax.rem(tp + n_tp - step, n_tp) * tok, tok)], gsr.at[step])
+        else:
+            far(c)
 
         def build(t, carry):
             r = at(t * part_rows, part_rows)
@@ -307,7 +340,7 @@
         def narrow(t, carry):
             r = at(t * part_rows, part_rows)
             td[r, :] = jnp.dot(
-                onehot[r, :], gm[0, :, at(tp * sub, sub)], preferred_element_type=F32
+                onehot[r, :], gs[...], preferred_element_type=F32
             ).astype(BF16)
             return carry
 
@@ -318,12 +351,10 @@
             lax.fori_loop(0, rows // part_rows, build, 0)
             spread(c, tx, rx, dts, drs)
 
-    forward(0)
     build_tables()
+    dispatch(0)
     forward(1)
-    own_chunk(2)
     attention_send(0)
-    dispatch(0)
     dispatch(1)
     forward(2)
     attention_send(1)
@@ -351,8 +382,15 @@
     narrow_own(td, rd, 0).wait()
     narrow_done(rd, ndr)
     my_slice = rx.at[0, :, at(tp * sub, sub)]
-    for step in range(1, n_tp):
-        send_tp(rd, my_slice, nxs.at[step], nxr.at[step], lax.rem(tp + step, n_tp))
+    send_tp(rd, my_slice, nxs.at[0], nxr.at[0], right)
+    send_tp(rd, my_slice, nxs.at[1], nxr.at[1], left)
+
+    def slice_of(who, half=None):
+        cols = at(who * sub, sub)
+        if half is None:
+            return rx.at[0, :, cols]
+        return rx.at[0, pl.ds(half * (rows // 2), rows // 2), cols]
+
     keep = pltpu.make_async_copy(rd, my_slice, nls.at[1])
     keep.start()
     dispatch(3)
@@ -366,6 +404,13 @@
     spans(across)
     late_load = pltpu.make_async_copy(wr_hbm, wa, wsem.at[13])
     late_load.start()
+    arrived(slice_of(left), nxr.at[0])
+    fwd = slice_of(left, 0)
+    send_tp(fwd, fwd, nxs.at[2], nxr.at[2], right)
+    arrived(slice_of(right), nxr.at[1])
+    fwd = slice_of(right, 1)
+    send_tp(fwd, fwd, nxs.at[3], nxr.at[3], left)
+    own_chunk(0)
     whole = neutral
     for m in range(n_tp):
         whole = after(whole, (blocks[m, 0], blocks[m, 1]))
@@ -440,6 +485,132 @@
         return ring_fold(4, zz, column)[0]
 
     in_chip, chip = level_one()
+    for copy in loads[9:11]:
+        copy.wait()
+    keep.wait()
+    arrived(slice_of(across, 0), nxr.at[2])
+    arrived(slice_of(across, 1), nxr.at[3])
+    for c in range(1, CHUNKS):
+        local_rows(c, tx, rx, dls).wait()
+        all_but_one(rx, c, drs)
+
+    loads[11].wait()
+    loads[12].wait()
+    narrow_done(td, nds)
+
+    def down(c):
+        def one(t, carry):
+            r = at(t * part_rows, part_rows)
+            tx[c, r, :] = jnp.dot(
+                hid[r, :], wd[:, c * wc : (c + 1) * wc], preferred_element_type=F32
+            ).astype(BF16)
+            return carry
+
+        lax.fori_loop(0, rows // part_rows, one, 0)
+
+    all_but_one(tx, 1, dts)
+    blocks_at_once = 8
+    cut = per // 3
+    planes = n_ep // blocks_at_once
+
+    def first_return(t, carry):
+        r = at(t * blocks_at_once * per, blocks_at_once * per)
+        both = []
+        for l in range(2):
+            g = jnp.zeros((blocks_at_once * 2 * cut, ffe), F32)
+            u = jnp.zeros((blocks_at_once * 2 * cut, ffe), F32)
+            for c in range(CHUNKS):
+                xs = rx[c, r, :].reshape(blocks_at_once, per, wc)[:, l * cut : (l + 2) * cut]
+                xs = xs.reshape(blocks_at_once * 2 * cut, wc)
+                g = g + jnp.dot(xs, wv[l, c * wc : (c + 1) * wc, :], preferred_element_type=F32)
+                u = u + jnp.dot(xs, wu[l, c * wc : (c + 1) * wc, :], preferred_element_type=F32)
+            h = jax.nn.silu(g) * u
+            ids = lax.rem(lax.broadcasted_iota(jnp.int32, h.shape, 0), 2 * cut)
+            h = jnp.where(ids >= per // 2 - cut if l else ids < per // 2, h, 0.0).astype(BF16)
+            h = h.reshape(blocks_at_once, 2 * cut, ffe)
+            empty = jnp.zeros((blocks_at_once, cut, ffe), BF16)
+            h = jnp.concatenate([empty, h] if l else [h, empty], axis=1)
+            both.append(h.reshape(blocks_at_once * per, ffe))
+        both = jnp.concatenate(both, axis=1)
+        hid[r, :] = both
+        tx[1, r, :] = jnp.dot(both, wd[:, wc : 2 * wc], preferred_element_type=F32).astype(BF16)
+
+        def one(i, carry):
+            k = t * blocks_at_once + i
+
+            @pl.when(k > 0)
+            def _():
+                to, here, there = ends(k, False)
+                pltpu.make_async_remote_copy(
+                    src_ref=tx.at[1, here],
+                    dst_ref=ry.at[0, there],
+                    send_sem=rts.at[1], recv_sem=rrs.at[1],
+                    device_id={"ep": to}, device_id_type=MESH,
+                ).start()
+
+            return carry
+
+        lax.fori_loop(0, blocks_at_once, one, 0)
+        return carry
+
+    in_column, column = level_two(chip)
+    lax.fori_loop(0, planes, first_return, 0)
+    local_rows(1, tx, ry, rls).start()
+    forward(0)
+
+    down(0)
+    for step in range(1, n_tp):
+        to = lax.rem(tp + step, n_tp)
+        cols = at(to * sub, sub)
+        send_tp(tx.at[0, :, cols], xr.at[step - 1], ros.at[step], ror.at[step], to)
+    all_but_one(tx, 2, dts)
+    down(2)
+    spread(2, tx, ry, rts, rrs)
+    all_but_one(tx, 3, dts)
+    down(3)
+
+    def weights(m, carry):
+        both = jnp.concatenate([metas[at(8 * m, 8), :], jnp.zeros((tok - 8, tok), F32)], axis=0).T
+        spot = both[:, 0:2].astype(jnp.int32)
+        for c in range(rows // 256):
+            ids = lax.broadcasted_iota(jnp.int32, (tok, 256), 1) + c * 256
+            w = jnp.where(ids == spot[:, 0:1], both[:, 2:3], 0.0) + jnp.where(
+                ids == spot[:, 1:2], both[:, 3:4], 0.0
+            )
+            weigh[at(m * tok, tok), c * 256 : (c + 1) * 256] = w.astype(BF16)
+        return carry
+
+    lax.fori_loop(0, n_tp, weights, 0)
+
+    in_slice = level_three(column)
+    earlier = after(after(in_slice, in_column), in_chip)
+
+    entering = earlier[1] + earlier[0] * first_ref[...]
+    for m in range(n_tp):
+        fade, held = blocks[m, 0], blocks[m, 1]
+        blocks[m, 1] = entering
+        entering = fade * entering + held
+
+    for step in range(n_tp):
+        who = lax.rem(tp + step + 1, n_tp)
+        wide_entry = jnp.concatenate([blocks[who, 1].astype(BF16)] * heads, axis=1) * vmask16
+
+        def finish(i, carry, who=who, wide_entry=wide_entry):
+            r = at(who * seg + i * 128, 128)
+            full = att[r, :] + jnp.dot(qg[r, :], wide_entry, preferred_element_type=F32)
+            for h in range(heads):
+                a = full[:, 128 * h : 128 * h + 128]
+                scale = lax.rsqrt(jnp.mean(a * a, axis=-1, keepdims=True) + NORM_EPS)
+                g = pj[r, 3 * kw + vw + 128 * h : 3 * kw + vw + 128 * h + 128].astype(F32)
+                gain = hgain_ref[:, 128 * h : 128 * h + 128]
+                pj[r, 128 * h : 128 * h + 128] = (a * scale * gain * jax.nn.silu(g)).astype(BF16)
+            return carry
+
+        lax.fori_loop(0, seg // 128, finish, 0)
+        if step < n_tp - 1:
+            send_tp(pj.at[at(who * seg, seg), 0:vw], pt.at[step], hs.at[step], hr.at[step], who)
+
+    far(0)
     loads[7].wait()
     loads[8].wait()
 
@@ -455,106 +626,12 @@
         return carry
 
     lax.fori_loop(0, n_tp, shared, 0)
-
-    for copy in loads[9:11]:
-        copy.wait()
-    keep.wait()
-    for step in range(1, n_tp):
-        arrived(rx.at[0, :, at(lax.rem(tp + n_tp - step, n_tp) * sub, sub)], nxr.at[step])
-    for c in range(1, CHUNKS):
-        local_rows(c, tx, rx, dls).wait()
-        all_but_one(rx, c, drs)
-
-    def expert(t, carry):
-        r = at(t * part_rows, part_rows)
-        late = lax.rem(lax.broadcasted_iota(jnp.int32, (part_rows, ffe), 0) + t * part_rows, 2 * slots) >= slots
-        for l in range(2):
-            g = jnp.zeros((part_rows, ffe), F32)
-            u = jnp.zeros((part_rows, ffe), F32)
-            for c in range(CHUNKS):
-                xs = rx[c, r, :]
-                g = g + jnp.dot(xs, wv[l, c * wc : (c + 1) * wc, :], preferred_element_type=F32)
-                u = u + jnp.dot(xs, wu[l, c * wc : (c + 1) * wc, :], preferred_element_type=F32)
-            h = jax.nn.silu(g) * u
-            h = jnp.where(late, h, 0.0) if l else jnp.where(late, 0.0, h)
-            hid[r, l * ffe : (l + 1) * ffe] = h.astype(BF16)
-        return carry
-
-    lax.fori_loop(0, rows // part_rows, expert, 0)
-    in_column, column = level_two(chip)
-
-    loads[11].wait()
-    loads[12].wait()
-    narrow_done(td, nds)
     for copy in gathers:
         copy.wait_send()
-
-    def down(c):
-        def one(t, carry):
-            r = at(t * part_rows, part_rows)
-            tx[c, r, :] = jnp.dot(
-                hid[r, :], wd[:, c * wc : (c + 1) * wc], preferred_element_type=F32
-            ).astype(BF16)
-            return carry
-
-        lax.fori_loop(0, rows // part_rows, one, 0)
-
-    all_but_one(tx, 1, dts)
-    down(1)
-    spread(1, tx, ry, rts, rrs)
-    down(0)
     gm[0, :, :] = jnp.dot(shid[...], jd[:, 0:wc], preferred_element_type=F32).astype(BF16)
     for step in range(1, n_tp):
         to = lax.rem(tp + step, n_tp)
-        cols = at(to * sub, sub)
-        send_tp(tx.at[0, :, cols], xr.at[step - 1], ros.at[step], ror.at[step], to)
-        send_tp(gm.at[0, :, cols], xs.at[step - 1], rcs.at[step], rcr.at[step], to)
-    all_but_one(tx, 2, dts)
-    down(2)
-    spread(2, tx, ry, rts, rrs)
-    all_but_one(tx, 3, dts)
-    down(3)
-
-    def weights(m, carry):
-        both = jnp.concatenate([metas[at(8 * m, 8), :], jnp.zeros((tok - 8, tok), F32)], axis=0).T
-        spot = both[:, 0:2].astype(jnp.int32)
-        for c in range(rows // 256):
-            ids = lax.broadcasted_iota(jnp.int32, (tok, 256), 1) + c * 256
-            w = jnp.where(ids == spot[:, 0:1], both[:, 2:3], 0.0) + jnp.where(
-                ids == spot[:, 1:2], both[:, 3:4], 0.0
-            )
-            weigh[at(m * tok, tok), c * 256 : (c + 1) * 256] = w.astype(BF16)
-        return carry
-
-    lax.fori_loop(0, n_tp, weights, 0)
-
-    in_slice = level_three(column)
-    earlier = after(after(in_slice, in_column), in_chip)
-
-    entering = earlier[1] + earlier[0] * first_ref[...]
-    for m in range(n_tp):
-        fade, held = blocks[m, 0], blocks[m, 1]
-        blocks[m, 1] = entering
-        entering = fade * entering + held
-
-    for step in range(n_tp):
-        who = lax.rem(tp + step + 1, n_tp)
-        wide_entry = jnp.concatenate([blocks[who, 1].astype(BF16)] * heads, axis=1) * vmask16
-
-        def finish(i, carry, who=who, wide_entry=wide_entry):
-            r = at(who * seg + i * 128, 128)
-            full = att[r, :] + jnp.dot(qg[r, :], wide_entry, preferred_element_type=F32)
-            for h in range(heads):
-                a = full[:, 128 * h : 128 * h + 128]
-                scale = lax.rsqrt(jnp.mean(a * a, axis=-1, keepdims=True) + NORM_EPS)
-                g = pj[r, 3 * kw + vw + 128 * h : 3 * kw + vw + 128 * h + 128].astype(F32)
-                gain = hgain_ref[:, 128 * h : 128 * h + 128]
-                pj[r, 128 * h : 128 * h + 128] = (a * scale * gain * jax.nn.silu(g)).astype(BF16)
-            return carry
-
-        lax.fori_loop(0, seg // 128, finish, 0)
-        if step < n_tp - 1:
-            send_tp(pj.at[at(who * seg, seg), 0:vw], pt.at[step], hs.at[step], hr.at[step], who)
+        send_tp(gm.at[0, :, at(to * sub, sub)], xs.at[step - 1], rcs.at[step], rcr.at[step], to)
 
     last = []
 
@@ -584,7 +661,6 @@
     collect(1)
     for step in range(1, n_tp):
         arrived(xr.at[step - 1], ror.at[step])
-        arrived(xs.at[step - 1], rcr.at[step])
 
     def slices(t, carry):
         r = at(t * 256, 256)
@@ -596,16 +672,16 @@
 
     lax.fori_loop(0, rows // 256, slices, 0)
     spread_narrow(td, rz, rzs, rzr, 2)
-    hc = wc // 2
+    parts = [(0, wc // 2), (wc // 2, wc // 4), (3 * wc // 4, wc // 4)]
 
     def spread_half(k):
-        cols = pl.ds(k * hc, hc)
+        cols = pl.ds(*parts[k])
 
         def one(i, carry):
-            to = peer(i)
+            to, here, there = ends(i, False)
             pltpu.make_async_remote_copy(
-                src_ref=tx.at[3, at(to * per, per), cols],
-                dst_ref=ry.at[2, at(ep * per, per), cols],
+                src_ref=tx.at[3, here, cols],
+                dst_ref=ry.at[2, there, cols],
                 send_sem=hts.at[k], recv_sem=hrs.at[k],
                 device_id={"ep": to}, device_id_type=MESH,
             ).start()
@@ -615,15 +691,15 @@
         half_own(k).start()
 
     def half_own(k):
-        own, cols = at(ep * per, per), pl.ds(k * hc, hc)
-        return pltpu.make_async_copy(tx.at[3, own, cols], ry.at[2, own, cols], hls.at[k])
+        own, cols = at(ep * per, per), pl.ds(*parts[k])
+        return pltpu.make_async_copy(tx.at[3, pl.ds(0, per), cols], ry.at[2, own, cols], hls.at[k])
 
     def half_done(ref, k, sem):
-        some = ref.at[pl.ds(0, rows - per), pl.ds(k * hc, hc)]
+        some = ref.at[pl.ds(0, rows - per), pl.ds(*parts[k])]
         pltpu.make_async_copy(some, some, sem.at[k]).wait()
 
-    spread_half(0)
-    spread_half(1)
+    for k in range(len(parts)):
+        spread_half(k)
     collect(2)
     late_load.wait()
     from_self = pj[at(tp * seg, seg), 0:vw]
@@ -643,6 +719,8 @@
 
     narrow_own(td, rz, 2).wait()
     narrow_done(rz, rzr)
+    for step in range(1, n_tp):
+        arrived(xs.at[step - 1], rcr.at[step])
     for m in range(n_tp):
         r = slice(m * tok, (m + 1) * tok)
         got = jnp.dot(weigh[r, :], rz[...], preferred_element_type=F32)
@@ -667,21 +745,23 @@
         half_own(k).wait()
         half_done(ry.at[2], k, hrs)
 
+        start, size = parts[k]
+
         def combine(m, carry):
             r = at(m * 256, 256)
-            got = jnp.dot(weigh[r, :], ry[2, :, k * hc : (k + 1) * hc], preferred_element_type=F32)
+            got = jnp.dot(weigh[r, :], ry[2, :, start : start + size], preferred_element_type=F32)
             got = got + jnp.dot(
-                shid[r, :], jd[:, 3 * wc + k * hc : 3 * wc + (k + 1) * hc], preferred_element_type=F32
+                shid[r, :], jd[:, 3 * wc + start : 3 * wc + start + size], preferred_element_type=F32
             )
-            gm[3, r, k * hc : (k + 1) * hc] = got.astype(BF16)
+            gm[3, r, start : start + size] = got.astype(BF16)
             return carry
 
         lax.fori_loop(0, n_tp * tok // 256, combine, 0)
         for step in range(1, n_tp):
             to = lax.rem(tp + step, n_tp)
             copy = pltpu.make_async_remote_copy(
-                src_ref=gm.at[3, at(to * tok, tok), pl.ds(k * hc, hc)],
-                dst_ref=fx.at[2, step - 1, :, pl.ds(k * hc, hc)],
+                src_ref=gm.at[3, at(to * tok, tok), pl.ds(start, size)],
+                dst_ref=fx.at[2, step - 1, :, pl.ds(start, size)],
                 send_sem=hfs.at[k, step], recv_sem=hfr.at[k, step],
                 device_id={"tp": to}, device_id_type=MESH,
             )
@@ -702,16 +782,17 @@
         final[step - 1].wait()
         moe_out[:, at(lax.rem(tp + n_tp - step, n_tp) * sub, sub)] = fz[step - 1]
     collect_half(1)
+    collect_half(2)
     for copy in sends:
         copy.wait_send()
 
-    for k in range(2):
-        cols = slice(k * hc, (k + 1) * hc)
+    for k, (start, size) in enumerate(parts):
+        cols = slice(start, start + size)
         total = gm[3, mine, cols].astype(F32)
         for step in range(1, n_tp):
             halves[k * (n_tp - 1) + step - 1].wait()
             total = total + fx[2, step - 1, :, cols].astype(F32)
-        moe_out[:, 3 * wc + k * hc : 3 * wc + (k + 1) * hc] = total.astype(BF16)
+        moe_out[:, 3 * wc + start : 3 * wc + start + size] = total.astype(BF16)
         half_done(tx.at[3], k, hts)
 
 
@@ -732,7 +813,7 @@
     vmem = pl.BlockSpec(memory_space=pltpu.VMEM)
     dma = pltpu.SemaphoreType.DMA
     V = pltpu.VMEM
-    return pl.pallas_call(
+    results = pl.pallas_call(
         functools.partial(layer_kernel, (n_ep, n_tp, tok, width, slots, ffe, seg, kw, vw)),
         out_shape=(
             jax.ShapeDtypeStruct((seg, width), BF16),
@@ -767,7 +848,7 @@
             V((CHUNKS - 1, n_tp - 1, tok, wc), BF16),
             V((rows, sub), BF16), V((rows, sub), BF16), V((rows, sub), BF16),
             V((n_tp - 1, rows, sub), BF16), V((n_tp - 1, n_tp * tok, sub), BF16),
-            V((n_tp * tok, sub), BF16), V((n_tp - 1, tok, sub), BF16),
+            V((n_tp * tok, sub), BF16), V((n_tp - 1, tok, sub), BF16), V((n_tp * tok, sub), BF16),
             dma((14,)), dma((CHUNKS, 4)), dma((CHUNKS, 4)), dma((n_tp,)), dma((n_tp,)),
             dma((CHUNKS,)), dma((CHUNKS,)), dma((CHUNKS,)),
             dma((CHUNKS,)), dma((CHUNKS,)), dma((CHUNKS,)),
@@ -775,7 +856,7 @@
             dma((3, 4)), dma((3, 4)), dma((7,)), dma((7,)), dma((n_tp,)), dma((n_tp,)),
             dma((1,)), dma((1,)), dma((n_tp,)), dma((n_tp,)), dma((n_tp,)), dma((n_tp,)), dma((n_tp,)), dma((n_tp,)),
             dma((1,)), dma((1,)), dma((n_tp,)), dma((n_tp,)), dma((3,)),
-            dma((2,)), dma((2,)), dma((2,)), dma((2, n_tp)), dma((2, n_tp)),
+            dma((3,)), dma((3,)), dma((3,)), dma((3, n_tp)), dma((3, n_tp)), dma((n_tp,)), dma((n_tp,)),
         ],
         compiler_params=pltpu.CompilerParams(
             collective_id=0, has_side_effects=True, vmem_limit_bytes=67043328
@@ -786,6 +867,25 @@
         hgain.reshape(1, -1), wr,
         x, gain.reshape(1, -1), picked.T, mixing.T, wv, wu, wd.reshape(2 * ffe, width), jv, ju, jd,
     )
+    return pl.pallas_call(
+        publish,
+        out_shape=tuple(jax.ShapeDtypeStruct(r.shape, r.dtype) for r in results),
+        in_specs=[vmem, vmem],
+        out_specs=(hbm, hbm),
+        scratch_shapes=[dma((2,))],
+        name="publish",
+    )(*results)
+
+
+def publish(mix_ref, moe_ref, mix_out, moe_out, sem):
+    copies = [
+        pltpu.make_async_copy(mix_ref, mix_out, sem.at[0]),
+        pltpu.make_async_copy(moe_ref, moe_out, sem.at[1]),
+    ]
+    for copy in copies:
+        copy.start()
+    for copy in copies:
+        copy.wait()
 
 
 def solution(mesh):

time: 175 us -> 151 us (0.86)
  Pallas kernels: 171 us -> 149 us
  local copies, waits for them, and re-layouts: 3.16 us -> 0 us
    pallas_call x1, Pallas kernels: 171 us -> 147 us  [body(): pl.pallas_call(functools.partial(layer_kernel, (n_ep, n_tp, tok, width, s...]
    unnamed x4 -> x0, local copies, waits for them, and re-layouts: 3.16 us -> none
    pallas_call x0 -> x1, Pallas kernels: none -> 2.51 us  [body(): pl.pallas_call(publish, out_shape=tuple((jax.ShapeDtypeStruct(r.shape, r....]
where the time goes in v2:
time: 151 us; the launch traced here: 150 us
  Pallas kernels  149 us (99%)
    pallas_call x1, Pallas kernels, body(): pl.pallas_call(functools.partial(layer_kernel, (n_ep, n_tp, tok, width, s...  147 us

profile of v2, /device:TPU:0, one launch (start us, length us, event | category | flops | bytes accessed | tf_op | source)
XLA Modules:
  0.0 150.0 jit_solution(3421827405063137019)
XLA Ops:
  0.6 146.7 %layer.1 = (bf16[256,2048]{1,0:T(8,128)(2,1)}, bf16[128,2048]{1,0:T(8,128)(2,1)}) custom-call(bf16[256,2048]{1,0:T(8,128)(2,1)} %xa_hbm.1, f32[1,2048]{1,0:T(1,128)} %bitcast.10, bf16[2048,256]{1,0:T(8,128)(2,1)} %wq_hbm.1, bf16[2048,256]{1,0:T(8,128)(2,1)} %wk_hbm.1, bf16[2048,256]{1,0:T(8,128)(2,1)} %wf_hbm.1, bf16[2048,512]{1,0:T(8,128)(2,1)} %wc_hbm.1, ...), custom_call_target="tpu_custom_call" | custom-call | tf_op jit(solution)/shard_map/layer/pallas_call | solution.py:816
  147.4 2.5 %publish.1 = (bf16[256,2048]{1,0:T(8,128)(2,1)}, bf16[128,2048]{1,0:T(8,128)(2,1)}) custom-call(bf16[256,2048]{1,0:T(8,128)(2,1)} %get-tuple-element.4.mix_ref, bf16[128,2048]{1,0:T(8,128)(2,1)} %get-tuple-element.5.moe_ref), custom_call_target="tpu_custom_call" | custom-call | tf_op jit(solution)/shard_map/publish/pallas_call | solution.py:870

commit v3 on v2

--- a/solution.py
+++ b/solution.py
@@ -569,6 +569,34 @@
     all_but_one(tx, 3, dts)
     down(3)
 
+    parts = [(0, wc // 2), (wc // 2, wc // 4), (3 * wc // 4, wc // 4)]
+
+    def spread_half(k):
+        cols = pl.ds(*parts[k])
+
+        def one(i, carry):
+            to, here, there = ends(i, False)
+            pltpu.make_async_remote_copy(
+                src_ref=tx.at[3, here, cols],
+                dst_ref=ry.at[2, there, cols],
+                send_sem=hts.at[k], recv_sem=hrs.at[k],
+                device_id={"ep": to}, device_id_type=MESH,
+            ).start()
+            return carry
+
+        lax.fori_loop(1, n_ep, one, 0)
+        half_own(k).start()
+
+    def half_own(k):
+        own, cols = at(ep * per, per), pl.ds(*parts[k])
+        return pltpu.make_async_copy(tx.at[3, pl.ds(0, per), cols], ry.at[2, own, cols], hls.at[k])
+
+    def half_done(ref, k, sem):
+        some = ref.at[pl.ds(0, rows - per), pl.ds(*parts[k])]
+        pltpu.make_async_copy(some, some, sem.at[k]).wait()
+
+    for k in range(len(parts)):
+        spread_half(k)
     def weights(m, carry):
         both = jnp.concatenate([metas[at(8 * m, 8), :], jnp.zeros((tok - 8, tok), F32)], axis=0).T
         spot = both[:, 0:2].astype(jnp.int32)
@@ -672,34 +700,6 @@
 
     lax.fori_loop(0, rows // 256, slices, 0)
     spread_narrow(td, rz, rzs, rzr, 2)
-    parts = [(0, wc // 2), (wc // 2, wc // 4), (3 * wc // 4, wc // 4)]
-
-    def spread_half(k):
-        cols = pl.ds(*parts[k])
-
-        def one(i, carry):
-            to, here, there = ends(i, False)
-            pltpu.make_async_remote_copy(
-                src_ref=tx.at[3, here, cols],
-                dst_ref=ry.at[2, there, cols],
-                send_sem=hts.at[k], recv_sem=hrs.at[k],
-                device_id={"ep": to}, device_id_type=MESH,
-            ).start()
-            return carry
-
-        lax.fori_loop(1, n_ep, one, 0)
-        half_own(k).start()
-
-    def half_own(k):
-        own, cols = at(ep * per, per), pl.ds(*parts[k])
-        return pltpu.make_async_copy(tx.at[3, pl.ds(0, per), cols], ry.at[2, own, cols], hls.at[k])
-
-    def half_done(ref, k, sem):
-        some = ref.at[pl.ds(0, rows - per), pl.ds(*parts[k])]
-        pltpu.make_async_copy(some, some, sem.at[k]).wait()
-
-    for k in range(len(parts)):
-        spread_half(k)
     collect(2)
     late_load.wait()
     from_self = pj[at(tp * seg, seg), 0:vw]

time: 151 us -> 158 us (1.046)
  Pallas kernels: 149 us -> 157 us
    pallas_call x1, Pallas kernels: 147 us -> 155 us  [body(): pl.pallas_call(functools.partial(layer_kernel, (n_ep, n_tp, tok, width, s...]
where the time goes in v3:
time: 158 us
  Pallas kernels  157 us (99%)
    pallas_call x1, Pallas kernels, body(): pl.pallas_call(functools.partial(layer_kernel, (n_ep, n_tp, tok, width, s...  155 us

profile of v3, /device:TPU:0, one launch (start us, length us, event | category | flops | bytes accessed | tf_op | source)
XLA Modules:
  0.0 158.1 jit_solution(6272635601499228534)
XLA Ops:
  0.6 154.8 %layer.1 = (bf16[256,2048]{1,0:T(8,128)(2,1)}, bf16[128,2048]{1,0:T(8,128)(2,1)}) custom-call(bf16[256,2048]{1,0:T(8,128)(2,1)} %xa_hbm.1, f32[1,2048]{1,0:T(1,128)} %bitcast.10, bf16[2048,256]{1,0:T(8,128)(2,1)} %wq_hbm.1, bf16[2048,256]{1,0:T(8,128)(2,1)} %wk_hbm.1, bf16[2048,256]{1,0:T(8,128)(2,1)} %wf_hbm.1, bf16[2048,512]{1,0:T(8,128)(2,1)} %wc_hbm.1, ...), custom_call_target="tpu_custom_call" | custom-call | tf_op jit(solution)/shard_map/layer/pallas_call | solution.py:816
  155.4 2.5 %publish.1 = (bf16[256,2048]{1,0:T(8,128)(2,1)}, bf16[128,2048]{1,0:T(8,128)(2,1)}) custom-call(bf16[256,2048]{1,0:T(8,128)(2,1)} %get-tuple-element.4.mix_ref, bf16[128,2048]{1,0:T(8,128)(2,1)} %get-tuple-element.5.moe_ref), custom_call_target="tpu_custom_call" | custom-call | tf_op jit(solution)/shard_map/publish/pallas_call | solution.py:870
